TPU v7x, 128 devices: a whole 4x4x4 slice. The times are simulated.
128 devices in a mesh: pp: 16 (over z, y), fs: 4 (over x), tp: 2 (over core).
Axes of the slice: x: 4, y: 4, z: 4, core: 2. Of those that a mesh axis runs over, the one named last changes fastest.
Arguments:
- tokens: bfloat16 [16, 8, 128, 2048], P('pp', ('fs', 'tp')), may hold values from -6 to 6
- layer_norm_scale: float32 [16, 2048], P('pp'), may hold values from 0.1 to 1.9
- input_weight: bfloat16 [16, 2048, 1024], P('pp'), may hold values from -0.125 to 0.125
- filter_weight: float32 [16, 4, 1024], P('pp'), may hold values from -3 to 3
- filter_bias: float32 [16, 1024], P('pp'), may hold values from -2 to 2
- recur_gate_weight: bfloat16 [16, 8, 128, 128], P('pp'), may hold values from -0.5 to 0.5
- recur_gate_bias: float32 [16, 1024], P('pp'), may hold values from -4 to 4
- input_gate_weight: bfloat16 [16, 8, 128, 128], P('pp'), may hold values from -0.5 to 0.5
- input_gate_bias: float32 [16, 1024], P('pp'), may hold values from -4 to 4
- decay_setting: float32 [16, 1024], P('pp'), may hold values from -2 to 8
- spike_log_decay: float32 [16, 128], P('pp'), may hold values from -0.7 to 0, as said below
- output_weight: bfloat16 [16, 1024, 2048], P('pp'), may hold values from -0.375 to 0.375
Outputs:
- result: bfloat16 [16, 8, 128, 2048], P('pp', ('fs', 'tp'))
Inputs may be any that keep to these rules, and one draw needn't show every extreme that they name: `spike_log_decay`: zero at most positions; at a few positions of each layer drawn from the seed it lies between log(0.5) and log(0.8).
All inputs are finite; a program needn't handle non-finite values.
Results may differ from a plain program's by a relative error of at most 0.023.
Values may be sent and summed in bfloat16 or wider, within the bound.
A program may use at most 64 MiB of HBM per device.

v0:
```python
import jax
import jax.numpy as jnp
from jax import lax
from jax.sharding import PartitionSpec as P


def from_behind(value, axis, by):
    devices = lax.axis_size(axis)
    return lax.ppermute(value, axis, [(i, (i + by) % devices) for i in range(devices)])


def combine_pair(left, right):
    return (left[0] * right[0], right[0] * left[1] + right[1])


def one_layer(hidden, weight_bundle):
    (
        norm_factor,
        input_projected,
        filter_kernel_taps,
        filter_offset,
        retention_weight,
        retention_bias,
        injection_weight,
        injection_bias,
        unscaled_decay,
        decay_spike,
        output_projected,
    ) = weight_bundle
    width = input_projected.shape[1]
    taps = filter_kernel_taps.shape[0]
    blocks = retention_weight.shape[0]
    length = hidden.shape[0]
    hidden32 = hidden.astype(jnp.float32)
    squares = jnp.mean(hidden32 * hidden32, axis=-1, keepdims=True)
    normed = (hidden32 * lax.rsqrt(squares + 1e-06) * norm_factor).astype(jnp.bfloat16)
    mixed_in = jnp.dot(normed, input_projected, preferred_element_type=jnp.float32).astype(
        jnp.bfloat16
    )
    padded = jnp.pad(mixed_in.astype(jnp.float32), ((taps - 1, 0), (0, 0)))
    conv_out = filter_offset + sum(
        (padded[k : k + length] * filter_kernel_taps[k] for k in range(taps))
    )
    conv_out = conv_out.astype(jnp.bfloat16)
    grouped = conv_out.reshape(length, blocks, -1)
    retention_gate = jax.nn.sigmoid(
        jnp.einsum(
            "ngi,gij->ngj", grouped, retention_weight, preferred_element_type=jnp.float32
        ).reshape(length, width)
        + retention_bias
    )
    inject = jax.nn.sigmoid(
        jnp.einsum(
            "ngi,gij->ngj", grouped, injection_weight, preferred_element_type=jnp.float32
        ).reshape(length, width)
        + injection_bias
    )
    decay_logarithm = (
        -8.0 * retention_gate * jax.nn.softplus(-unscaled_decay) + decay_spike[:, None]
    )
    decay = jnp.exp(decay_logarithm)
    update = jnp.sqrt(-jnp.expm1(2.0 * decay_logarithm)) * inject * conv_out.astype(jnp.float32)
    states = lax.associative_scan(combine_pair, (decay, update), axis=0)[1].astype(jnp.bfloat16)
    projected = jnp.dot(states, output_projected, preferred_element_type=jnp.float32)
    return (hidden32 + projected).astype(jnp.bfloat16)


def local(
    tokens,
    layer_norm_scale,
    input_weight,
    filter_weight,
    filter_bias,
    recur_gate_weight,
    recur_gate_bias,
    input_gate_weight,
    input_gate_bias,
    decay_setting,
    spike_log_decay,
    output_weight,
):
    sections = lax.axis_size("pp")
    section_id = lax.axis_index("pp")
    weight_bundle = (
        layer_norm_scale[0],
        input_weight[0],
        filter_weight[0],
        filter_bias[0],
        recur_gate_weight[0],
        recur_gate_bias[0],
        input_gate_weight[0],
        input_gate_bias[0],
        decay_setting[0],
        spike_log_decay[0],
        output_weight[0],
    )
    initial = tokens[0, 0]

    def run_layer(activations):
        return one_layer(activations, weight_bundle)

    def passed(activations):
        return activations

    def advance(moment, carried):
        active = (moment >= section_id) & (moment < section_id + sections)
        layered = lax.cond(active, run_layer, passed, carried)
        return from_behind(layered, "pp", 1)

    finished = lax.fori_loop(0, 2 * sections, advance, initial)
    return finished[None, None]


def solution(mesh):
    placed = (
        P("pp", ("fs", "tp"), None, None),
        P("pp", None),
        P("pp", None, None),
        P("pp", None, None),
        P("pp", None),
        P("pp", None, None, None),
        P("pp", None),
        P("pp", None, None, None),
        P("pp", None),
        P("pp", None),
        P("pp", None),
        P("pp", None, None),
    )
    return jax.shard_map(
        local,
        mesh=mesh,
        in_specs=placed,
        out_specs=P("pp", ("fs", "tp"), None, None),
        check_vma=False,
    )
```

profile of v0, /device:TPU:4, one launch (start us, length us, event | category | flops | bytes accessed | tf_op | source)
XLA Modules:
  0.0 859.1 jit_solution(11305456885782503485)
XLA Ops:
  4.0 854.3 %while.17 = (s32[]{:T(128)}, bf16[128,2048]{1,0:T(8,128)(2,1)S(1)}, s32[]{:T(128)}, s32[]{:T(128)}, f32[1,1024]{1,0:T(1,128)}, /*index=5*/f32[1,2048]{1,0:T(1,12...) while((s32[]{:T(128)}, bf16[128,2048]{1,0:T(8,128)(2,1)S(1)}, ...), condition=%wide.region_4.5_spmd, body=%wide.region_0.4_spmd.sunk | while | flops 1149344896 | bytes 40322016 | solution.py:110
  4.0 14.1 %conditional.2 = (bf16[128,2048]{1,0:T(8,128)(2,1)S(1)}) conditional(s32[]{:T(128)} %convert_element_type.60, bf16[128,2048]{1,0:T(8,128)(2,1)S(1)} %get-tuple-element.499, (bf16[128,2048]{1,0:T(8,128)(2,1)S(1)}, f32[1,1024]{1,0:T(1,128)}, f32[1,2048]{1,0:T(1,128)}, bf16[2048,1024]{1,0:T(8,128)(2,1)}, f32[4,1024]{1,0:T(4,128)}, ...), branch_computations={%region_1.0_spmd, %region_2.3_spmd} | conditional | flops 1149344896 | bytes 37175976 | solution.py:107
  15.0 3.1 fusion
  18.2 17.0 %collective-permute-done = bf16[128,2048]{1,0:T(8,128)(2,1)S(1)} collective-permute-done((bf16[128,2048]{1,0:T(8,128)(2,1)S(1)}, bf16[128,2048]{1,0:T(8,128)(2,1)S(1)}, u32[]{:S(2)}, u32[]{:S(2)}) %collective-permute-start) | collective-permute-done | bytes 524320 | tf_op jit(solution)/shard_map/while/body/eval_jaxpr/ppermute | solution.py:9
  35.2 14.1 %conditional.2 = (bf16[128,2048]{1,0:T(8,128)(2,1)S(1)}) conditional(s32[]{:T(128)} %convert_element_type.60, bf16[128,2048]{1,0:T(8,128)(2,1)S(1)} %get-tuple-element.499, (bf16[128,2048]{1,0:T(8,128)(2,1)S(1)}, f32[1,1024]{1,0:T(1,128)}, f32[1,2048]{1,0:T(1,128)}, bf16[2048,1024]{1,0:T(8,128)(2,1)}, f32[4,1024]{1,0:T(4,128)}, ...), branch_computations={%region_1.0_spmd, %region_2.3_spmd} | conditional | flops 1149344896 | bytes 37175976 | solution.py:107
  46.3 3.1 fusion
  49.5 16.1 %collective-permute-done = bf16[128,2048]{1,0:T(8,128)(2,1)S(1)} collective-permute-done((bf16[128,2048]{1,0:T(8,128)(2,1)S(1)}, bf16[128,2048]{1,0:T(8,128)(2,1)S(1)}, u32[]{:S(2)}, u32[]{:S(2)}) %collective-permute-start) | collective-permute-done | bytes 524320 | tf_op jit(solution)/shard_map/while/body/eval_jaxpr/ppermute | solution.py:9
  65.6 14.1 %conditional.2 = (bf16[128,2048]{1,0:T(8,128)(2,1)S(1)}) conditional(s32[]{:T(128)} %convert_element_type.60, bf16[128,2048]{1,0:T(8,128)(2,1)S(1)} %get-tuple-element.499, (bf16[128,2048]{1,0:T(8,128)(2,1)S(1)}, f32[1,1024]{1,0:T(1,128)}, f32[1,2048]{1,0:T(1,128)}, bf16[2048,1024]{1,0:T(8,128)(2,1)}, f32[4,1024]{1,0:T(4,128)}, ...), branch_computations={%region_1.0_spmd, %region_2.3_spmd} | conditional | flops 1149344896 | bytes 37175976 | solution.py:107
  79.9 15.3 %collective-permute-done = bf16[128,2048]{1,0:T(8,128)(2,1)S(1)} collective-permute-done((bf16[128,2048]{1,0:T(8,128)(2,1)S(1)}, bf16[128,2048]{1,0:T(8,128)(2,1)S(1)}, u32[]{:S(2)}, u32[]{:S(2)}) %collective-permute-start) | collective-permute-done | bytes 524320 | tf_op jit(solution)/shard_map/while/body/eval_jaxpr/ppermute | solution.py:9
  95.2 14.1 %conditional.2 = (bf16[128,2048]{1,0:T(8,128)(2,1)S(1)}) conditional(s32[]{:T(128)} %convert_element_type.60, bf16[128,2048]{1,0:T(8,128)(2,1)S(1)} %get-tuple-element.499, (bf16[128,2048]{1,0:T(8,128)(2,1)S(1)}, f32[1,1024]{1,0:T(1,128)}, f32[1,2048]{1,0:T(1,128)}, bf16[2048,1024]{1,0:T(8,128)(2,1)}, f32[4,1024]{1,0:T(4,128)}, ...), branch_computations={%region_1.0_spmd, %region_2.3_spmd} | conditional | flops 1149344896 | bytes 37175976 | solution.py:107
  109.4 14.4 %collective-permute-done = bf16[128,2048]{1,0:T(8,128)(2,1)S(1)} collective-permute-done((bf16[128,2048]{1,0:T(8,128)(2,1)S(1)}, bf16[128,2048]{1,0:T(8,128)(2,1)S(1)}, u32[]{:S(2)}, u32[]{:S(2)}) %collective-permute-start) | collective-permute-done | bytes 524320 | tf_op jit(solution)/shard_map/while/body/eval_jaxpr/ppermute | solution.py:9
  123.9 14.1 %conditional.2 = (bf16[128,2048]{1,0:T(8,128)(2,1)S(1)}) conditional(s32[]{:T(128)} %convert_element_type.60, bf16[128,2048]{1,0:T(8,128)(2,1)S(1)} %get-tuple-element.499, (bf16[128,2048]{1,0:T(8,128)(2,1)S(1)}, f32[1,1024]{1,0:T(1,128)}, f32[1,2048]{1,0:T(1,128)}, bf16[2048,1024]{1,0:T(8,128)(2,1)}, f32[4,1024]{1,0:T(4,128)}, ...), branch_computations={%region_1.0_spmd, %region_2.3_spmd} | conditional | flops 1149344896 | bytes 37175976 | solution.py:107
  135.0 3.1 fusion
  138.1 13.6 %collective-permute-done = bf16[128,2048]{1,0:T(8,128)(2,1)S(1)} collective-permute-done((bf16[128,2048]{1,0:T(8,128)(2,1)S(1)}, bf16[128,2048]{1,0:T(8,128)(2,1)S(1)}, u32[]{:S(2)}, u32[]{:S(2)}) %collective-permute-start) | collective-permute-done | bytes 524320 | tf_op jit(solution)/shard_map/while/body/eval_jaxpr/ppermute | solution.py:9
  151.8 14.1 %conditional.2 = (bf16[128,2048]{1,0:T(8,128)(2,1)S(1)}) conditional(s32[]{:T(128)} %convert_element_type.60, bf16[128,2048]{1,0:T(8,128)(2,1)S(1)} %get-tuple-element.499, (bf16[128,2048]{1,0:T(8,128)(2,1)S(1)}, f32[1,1024]{1,0:T(1,128)}, f32[1,2048]{1,0:T(1,128)}, bf16[2048,1024]{1,0:T(8,128)(2,1)}, f32[4,1024]{1,0:T(4,128)}, ...), branch_computations={%region_1.0_spmd, %region_2.3_spmd} | conditional | flops 1149344896 | bytes 37175976 | solution.py:107
  162.8 3.1 fusion
  166.0 12.7 %collective-permute-done = bf16[128,2048]{1,0:T(8,128)(2,1)S(1)} collective-permute-done((bf16[128,2048]{1,0:T(8,128)(2,1)S(1)}, bf16[128,2048]{1,0:T(8,128)(2,1)S(1)}, u32[]{:S(2)}, u32[]{:S(2)}) %collective-permute-start) | collective-permute-done | bytes 524320 | tf_op jit(solution)/shard_map/while/body/eval_jaxpr/ppermute | solution.py:9
  178.8 14.1 %conditional.2 = (bf16[128,2048]{1,0:T(8,128)(2,1)S(1)}) conditional(s32[]{:T(128)} %convert_element_type.60, bf16[128,2048]{1,0:T(8,128)(2,1)S(1)} %get-tuple-element.499, (bf16[128,2048]{1,0:T(8,128)(2,1)S(1)}, f32[1,1024]{1,0:T(1,128)}, f32[1,2048]{1,0:T(1,128)}, bf16[2048,1024]{1,0:T(8,128)(2,1)}, f32[4,1024]{1,0:T(4,128)}, ...), branch_computations={%region_1.0_spmd, %region_2.3_spmd} | conditional | flops 1149344896 | bytes 37175976 | solution.py:107
  189.8 3.1 fusion
  193.0 12.5 %collective-permute-done = bf16[128,2048]{1,0:T(8,128)(2,1)S(1)} collective-permute-done((bf16[128,2048]{1,0:T(8,128)(2,1)S(1)}, bf16[128,2048]{1,0:T(8,128)(2,1)S(1)}, u32[]{:S(2)}, u32[]{:S(2)}) %collective-permute-start) | collective-permute-done | bytes 524320 | tf_op jit(solution)/shard_map/while/body/eval_jaxpr/ppermute | solution.py:9
  205.5 14.1 %conditional.2 = (bf16[128,2048]{1,0:T(8,128)(2,1)S(1)}) conditional(s32[]{:T(128)} %convert_element_type.60, bf16[128,2048]{1,0:T(8,128)(2,1)S(1)} %get-tuple-element.499, (bf16[128,2048]{1,0:T(8,128)(2,1)S(1)}, f32[1,1024]{1,0:T(1,128)}, f32[1,2048]{1,0:T(1,128)}, bf16[2048,1024]{1,0:T(8,128)(2,1)}, f32[4,1024]{1,0:T(4,128)}, ...), branch_computations={%region_1.0_spmd, %region_2.3_spmd} | conditional | flops 1149344896 | bytes 37175976 | solution.py:107
  216.6 3.1 fusion
  219.8 12.5 %collective-permute-done = bf16[128,2048]{1,0:T(8,128)(2,1)S(1)} collective-permute-done((bf16[128,2048]{1,0:T(8,128)(2,1)S(1)}, bf16[128,2048]{1,0:T(8,128)(2,1)S(1)}, u32[]{:S(2)}, u32[]{:S(2)}) %collective-permute-start) | collective-permute-done | bytes 524320 | tf_op jit(solution)/shard_map/while/body/eval_jaxpr/ppermute | solution.py:9
  232.3 14.1 %conditional.2 = (bf16[128,2048]{1,0:T(8,128)(2,1)S(1)}) conditional(s32[]{:T(128)} %convert_element_type.60, bf16[128,2048]{1,0:T(8,128)(2,1)S(1)} %get-tuple-element.499, (bf16[128,2048]{1,0:T(8,128)(2,1)S(1)}, f32[1,1024]{1,0:T(1,128)}, f32[1,2048]{1,0:T(1,128)}, bf16[2048,1024]{1,0:T(8,128)(2,1)}, f32[4,1024]{1,0:T(4,128)}, ...), branch_computations={%region_1.0_spmd, %region_2.3_spmd} | conditional | flops 1149344896 | bytes 37175976 | solution.py:107
  243.4 3.1 fusion
  246.6 12.5 %collective-permute-done = bf16[128,2048]{1,0:T(8,128)(2,1)S(1)} collective-permute-done((bf16[128,2048]{1,0:T(8,128)(2,1)S(1)}, bf16[128,2048]{1,0:T(8,128)(2,1)S(1)}, u32[]{:S(2)}, u32[]{:S(2)}) %collective-permute-start) | collective-permute-done | bytes 524320 | tf_op jit(solution)/shard_map/while/body/eval_jaxpr/ppermute | solution.py:9
  259.1 14.1 %conditional.2 = (bf16[128,2048]{1,0:T(8,128)(2,1)S(1)}) conditional(s32[]{:T(128)} %convert_element_type.60, bf16[128,2048]{1,0:T(8,128)(2,1)S(1)} %get-tuple-element.499, (bf16[128,2048]{1,0:T(8,128)(2,1)S(1)}, f32[1,1024]{1,0:T(1,128)}, f32[1,2048]{1,0:T(1,128)}, bf16[2048,1024]{1,0:T(8,128)(2,1)}, f32[4,1024]{1,0:T(4,128)}, ...), branch_computations={%region_1.0_spmd, %region_2.3_spmd} | conditional | flops 1149344896 | bytes 37175976 | solution.py:107
  270.2 3.1 fusion
  273.4 12.5 %collective-permute-done = bf16[128,2048]{1,0:T(8,128)(2,1)S(1)} collective-permute-done((bf16[128,2048]{1,0:T(8,128)(2,1)S(1)}, bf16[128,2048]{1,0:T(8,128)(2,1)S(1)}, u32[]{:S(2)}, u32[]{:S(2)}) %collective-permute-start) | collective-permute-done | bytes 524320 | tf_op jit(solution)/shard_map/while/body/eval_jaxpr/ppermute | solution.py:9
  285.9 14.1 %conditional.2 = (bf16[128,2048]{1,0:T(8,128)(2,1)S(1)}) conditional(s32[]{:T(128)} %convert_element_type.60, bf16[128,2048]{1,0:T(8,128)(2,1)S(1)} %get-tuple-element.499, (bf16[128,2048]{1,0:T(8,128)(2,1)S(1)}, f32[1,1024]{1,0:T(1,128)}, f32[1,2048]{1,0:T(1,128)}, bf16[2048,1024]{1,0:T(8,128)(2,1)}, f32[4,1024]{1,0:T(4,128)}, ...), branch_computations={%region_1.0_spmd, %region_2.3_spmd} | conditional | flops 1149344896 | bytes 37175976 | solution.py:107
  297.0 3.1 fusion
  300.1 12.5 %collective-permute-done = bf16[128,2048]{1,0:T(8,128)(2,1)S(1)} collective-permute-done((bf16[128,2048]{1,0:T(8,128)(2,1)S(1)}, bf16[128,2048]{1,0:T(8,128)(2,1)S(1)}, u32[]{:S(2)}, u32[]{:S(2)}) %collective-permute-start) | collective-permute-done | bytes 524320 | tf_op jit(solution)/shard_map/while/body/eval_jaxpr/ppermute | solution.py:9
  312.7 14.1 %conditional.2 = (bf16[128,2048]{1,0:T(8,128)(2,1)S(1)}) conditional(s32[]{:T(128)} %convert_element_type.60, bf16[128,2048]{1,0:T(8,128)(2,1)S(1)} %get-tuple-element.499, (bf16[128,2048]{1,0:T(8,128)(2,1)S(1)}, f32[1,1024]{1,0:T(1,128)}, f32[1,2048]{1,0:T(1,128)}, bf16[2048,1024]{1,0:T(8,128)(2,1)}, f32[4,1024]{1,0:T(4,128)}, ...), branch_computations={%region_1.0_spmd, %region_2.3_spmd} | conditional | flops 1149344896 | bytes 37175976 | solution.py:107
  323.8 3.1 fusion
  326.9 12.5 %collective-permute-done = bf16[128,2048]{1,0:T(8,128)(2,1)S(1)} collective-permute-done((bf16[128,2048]{1,0:T(8,128)(2,1)S(1)}, bf16[128,2048]{1,0:T(8,128)(2,1)S(1)}, u32[]{:S(2)}, u32[]{:S(2)}) %collective-permute-start) | collective-permute-done | bytes 524320 | tf_op jit(solution)/shard_map/while/body/eval_jaxpr/ppermute | solution.py:9
  339.5 14.1 %conditional.2 = (bf16[128,2048]{1,0:T(8,128)(2,1)S(1)}) conditional(s32[]{:T(128)} %convert_element_type.60, bf16[128,2048]{1,0:T(8,128)(2,1)S(1)} %get-tuple-element.499, (bf16[128,2048]{1,0:T(8,128)(2,1)S(1)}, f32[1,1024]{1,0:T(1,128)}, f32[1,2048]{1,0:T(1,128)}, bf16[2048,1024]{1,0:T(8,128)(2,1)}, f32[4,1024]{1,0:T(4,128)}, ...), branch_computations={%region_1.0_spmd, %region_2.3_spmd} | conditional | flops 1149344896 | bytes 37175976 | solution.py:107
  350.6 3.1 fusion
  353.7 12.5 %collective-permute-done = bf16[128,2048]{1,0:T(8,128)(2,1)S(1)} collective-permute-done((bf16[128,2048]{1,0:T(8,128)(2,1)S(1)}, bf16[128,2048]{1,0:T(8,128)(2,1)S(1)}, u32[]{:S(2)}, u32[]{:S(2)}) %collective-permute-start) | collective-permute-done | bytes 524320 | tf_op jit(solution)/shard_map/while/body/eval_jaxpr/ppermute | solution.py:9
  366.3 14.1 %conditional.2 = (bf16[128,2048]{1,0:T(8,128)(2,1)S(1)}) conditional(s32[]{:T(128)} %convert_element_type.60, bf16[128,2048]{1,0:T(8,128)(2,1)S(1)} %get-tuple-element.499, (bf16[128,2048]{1,0:T(8,128)(2,1)S(1)}, f32[1,1024]{1,0:T(1,128)}, f32[1,2048]{1,0:T(1,128)}, bf16[2048,1024]{1,0:T(8,128)(2,1)}, f32[4,1024]{1,0:T(4,128)}, ...), branch_computations={%region_1.0_spmd, %region_2.3_spmd} | conditional | flops 1149344896 | bytes 37175976 | solution.py:107
  377.3 3.1 fusion
  380.5 12.5 %collective-permute-done = bf16[128,2048]{1,0:T(8,128)(2,1)S(1)} collective-permute-done((bf16[128,2048]{1,0:T(8,128)(2,1)S(1)}, bf16[128,2048]{1,0:T(8,128)(2,1)S(1)}, u32[]{:S(2)}, u32[]{:S(2)}) %collective-permute-start) | collective-permute-done | bytes 524320 | tf_op jit(solution)/shard_map/while/body/eval_jaxpr/ppermute | solution.py:9
  393.1 14.1 %conditional.2 = (bf16[128,2048]{1,0:T(8,128)(2,1)S(1)}) conditional(s32[]{:T(128)} %convert_element_type.60, bf16[128,2048]{1,0:T(8,128)(2,1)S(1)} %get-tuple-element.499, (bf16[128,2048]{1,0:T(8,128)(2,1)S(1)}, f32[1,1024]{1,0:T(1,128)}, f32[1,2048]{1,0:T(1,128)}, bf16[2048,1024]{1,0:T(8,128)(2,1)}, f32[4,1024]{1,0:T(4,128)}, ...), branch_computations={%region_1.0_spmd, %region_2.3_spmd} | conditional | flops 1149344896 | bytes 37175976 | solution.py:107
  404.1 3.1 fusion
  407.3 12.5 %collective-permute-done = bf16[128,2048]{1,0:T(8,128)(2,1)S(1)} collective-permute-done((bf16[128,2048]{1,0:T(8,128)(2,1)S(1)}, bf16[128,2048]{1,0:T(8,128)(2,1)S(1)}, u32[]{:S(2)}, u32[]{:S(2)}) %collective-permute-start) | collective-permute-done | bytes 524320 | tf_op jit(solution)/shard_map/while/body/eval_jaxpr/ppermute | solution.py:9
  419.8 14.1 %conditional.2 = (bf16[128,2048]{1,0:T(8,128)(2,1)S(1)}) conditional(s32[]{:T(128)} %convert_element_type.60, bf16[128,2048]{1,0:T(8,128)(2,1)S(1)} %get-tuple-element.499, (bf16[128,2048]{1,0:T(8,128)(2,1)S(1)}, f32[1,1024]{1,0:T(1,128)}, f32[1,2048]{1,0:T(1,128)}, bf16[2048,1024]{1,0:T(8,128)(2,1)}, f32[4,1024]{1,0:T(4,128)}, ...), branch_computations={%region_1.0_spmd, %region_2.3_spmd} | conditional | flops 1149344896 | bytes 37175976 | solution.py:107
  430.9 3.1 fusion
  434.1 14.2 %collective-permute-done = bf16[128,2048]{1,0:T(8,128)(2,1)S(1)} collective-permute-done((bf16[128,2048]{1,0:T(8,128)(2,1)S(1)}, bf16[128,2048]{1,0:T(8,128)(2,1)S(1)}, u32[]{:S(2)}, u32[]{:S(2)}) %collective-permute-start) | collective-permute-done | bytes 524320 | tf_op jit(solution)/shard_map/while/body/eval_jaxpr/ppermute | solution.py:9
  448.4 9.1 %collective-permute-start = (bf16[128,2048]{1,0:T(8,128)(2,1)S(1)}, bf16[128,2048]{1,0:T(8,128)(2,1)S(1)}, u32[]{:S(2)}, u32[]{:S(2)}) collective-permute-start(bf16[128,2048]{1,0:T(8,128)(2,1)S(1)} %get-tuple-element.530), channel_id=1, source_target_pairs={{0,8},{8,16},{16,24},{24,32},{32,40},{40,48},{48,56},{56,64},{64,7... | collective-permute-start | bytes 1572872 | tf_op jit(solution)/shard_map/while/body/eval_jaxpr/ppermute | solution.py:9
  457.5 14.0 %collective-permute-done = bf16[128,2048]{1,0:T(8,128)(2,1)S(1)} collective-permute-done((bf16[128,2048]{1,0:T(8,128)(2,1)S(1)}, bf16[128,2048]{1,0:T(8,128)(2,1)S(1)}, u32[]{:S(2)}, u32[]{:S(2)}) %collective-permute-start) | collective-permute-done | bytes 524320 | tf_op jit(solution)/shard_map/while/body/eval_jaxpr/ppermute | solution.py:9
  471.7 27.0 %collective-permute-done = bf16[128,2048]{1,0:T(8,128)(2,1)S(1)} collective-permute-done((bf16[128,2048]{1,0:T(8,128)(2,1)S(1)}, bf16[128,2048]{1,0:T(8,128)(2,1)S(1)}, u32[]{:S(2)}, u32[]{:S(2)}) %collective-permute-start) | collective-permute-done | bytes 524320 | tf_op jit(solution)/shard_map/while/body/eval_jaxpr/ppermute | solution.py:9
  498.8 28.1 %collective-permute-done = bf16[128,2048]{1,0:T(8,128)(2,1)S(1)} collective-permute-done((bf16[128,2048]{1,0:T(8,128)(2,1)S(1)}, bf16[128,2048]{1,0:T(8,128)(2,1)S(1)}, u32[]{:S(2)}, u32[]{:S(2)}) %collective-permute-start) | collective-permute-done | bytes 524320 | tf_op jit(solution)/shard_map/while/body/eval_jaxpr/ppermute | solution.py:9
  527.1 29.1 %collective-permute-done = bf16[128,2048]{1,0:T(8,128)(2,1)S(1)} collective-permute-done((bf16[128,2048]{1,0:T(8,128)(2,1)S(1)}, bf16[128,2048]{1,0:T(8,128)(2,1)S(1)}, u32[]{:S(2)}, u32[]{:S(2)}) %collective-permute-start) | collective-permute-done | bytes 524320 | tf_op jit(solution)/shard_map/while/body/eval_jaxpr/ppermute | solution.py:9
  556.4 27.7 %collective-permute-done = bf16[128,2048]{1,0:T(8,128)(2,1)S(1)} collective-permute-done((bf16[128,2048]{1,0:T(8,128)(2,1)S(1)}, bf16[128,2048]{1,0:T(8,128)(2,1)S(1)}, u32[]{:S(2)}, u32[]{:S(2)}) %collective-permute-start) | collective-permute-done | bytes 524320 | tf_op jit(solution)/shard_map/while/body/eval_jaxpr/ppermute | solution.py:9
  584.3 26.9 %collective-permute-done = bf16[128,2048]{1,0:T(8,128)(2,1)S(1)} collective-permute-done((bf16[128,2048]{1,0:T(8,128)(2,1)S(1)}, bf16[128,2048]{1,0:T(8,128)(2,1)S(1)}, u32[]{:S(2)}, u32[]{:S(2)}) %collective-permute-start) | collective-permute-done | bytes 524320 | tf_op jit(solution)/shard_map/while/body/eval_jaxpr/ppermute | solution.py:9
  611.3 26.0 %collective-permute-done = bf16[128,2048]{1,0:T(8,128)(2,1)S(1)} collective-permute-done((bf16[128,2048]{1,0:T(8,128)(2,1)S(1)}, bf16[128,2048]{1,0:T(8,128)(2,1)S(1)}, u32[]{:S(2)}, u32[]{:S(2)}) %collective-permute-start) | collective-permute-done | bytes 524320 | tf_op jit(solution)/shard_map/while/body/eval_jaxpr/ppermute | solution.py:9
  637.5 25.1 %collective-permute-done = bf16[128,2048]{1,0:T(8,128)(2,1)S(1)} collective-permute-done((bf16[128,2048]{1,0:T(8,128)(2,1)S(1)}, bf16[128,2048]{1,0:T(8,128)(2,1)S(1)}, u32[]{:S(2)}, u32[]{:S(2)}) %collective-permute-start) | collective-permute-done | bytes 524320 | tf_op jit(solution)/shard_map/while/body/eval_jaxpr/ppermute | solution.py:9
  662.8 24.3 %collective-permute-done = bf16[128,2048]{1,0:T(8,128)(2,1)S(1)} collective-permute-done((bf16[128,2048]{1,0:T(8,128)(2,1)S(1)}, bf16[128,2048]{1,0:T(8,128)(2,1)S(1)}, u32[]{:S(2)}, u32[]{:S(2)}) %collective-permute-start) | collective-permute-done | bytes 524320 | tf_op jit(solution)/shard_map/while/body/eval_jaxpr/ppermute | solution.py:9
  687.2 27.5 %collective-permute-done = bf16[128,2048]{1,0:T(8,128)(2,1)S(1)} collective-permute-done((bf16[128,2048]{1,0:T(8,128)(2,1)S(1)}, bf16[128,2048]{1,0:T(8,128)(2,1)S(1)}, u32[]{:S(2)}, u32[]{:S(2)}) %collective-permute-start) | collective-permute-done | bytes 524320 | tf_op jit(solution)/shard_map/while/body/eval_jaxpr/ppermute | solution.py:9
  714.9 25.4 %collective-permute-done = bf16[128,2048]{1,0:T(8,128)(2,1)S(1)} collective-permute-done((bf16[128,2048]{1,0:T(8,128)(2,1)S(1)}, bf16[128,2048]{1,0:T(8,128)(2,1)S(1)}, u32[]{:S(2)}, u32[]{:S(2)}) %collective-permute-start) | collective-permute-done | bytes 524320 | tf_op jit(solution)/shard_map/while/body/eval_jaxpr/ppermute | solution.py:9
  740.4 24.5 %collective-permute-done = bf16[128,2048]{1,0:T(8,128)(2,1)S(1)} collective-permute-done((bf16[128,2048]{1,0:T(8,128)(2,1)S(1)}, bf16[128,2048]{1,0:T(8,128)(2,1)S(1)}, u32[]{:S(2)}, u32[]{:S(2)}) %collective-permute-start) | collective-permute-done | bytes 524320 | tf_op jit(solution)/shard_map/while/body/eval_jaxpr/ppermute | solution.py:9
  765.1 24.4 %collective-permute-done = bf16[128,2048]{1,0:T(8,128)(2,1)S(1)} collective-permute-done((bf16[128,2048]{1,0:T(8,128)(2,1)S(1)}, bf16[128,2048]{1,0:T(8,128)(2,1)S(1)}, u32[]{:S(2)}, u32[]{:S(2)}) %collective-permute-start) | collective-permute-done | bytes 524320 | tf_op jit(solution)/shard_map/while/body/eval_jaxpr/ppermute | solution.py:9
  789.7 26.6 %collective-permute-done = bf16[128,2048]{1,0:T(8,128)(2,1)S(1)} collective-permute-done((bf16[128,2048]{1,0:T(8,128)(2,1)S(1)}, bf16[128,2048]{1,0:T(8,128)(2,1)S(1)}, u32[]{:S(2)}, u32[]{:S(2)}) %collective-permute-start) | collective-permute-done | bytes 524320 | tf_op jit(solution)/shard_map/while/body/eval_jaxpr/ppermute | solution.py:9
  816.5 29.1 %collective-permute-done = bf16[128,2048]{1,0:T(8,128)(2,1)S(1)} collective-permute-done((bf16[128,2048]{1,0:T(8,128)(2,1)S(1)}, bf16[128,2048]{1,0:T(8,128)(2,1)S(1)}, u32[]{:S(2)}, u32[]{:S(2)}) %collective-permute-start) | collective-permute-done | bytes 524320 | tf_op jit(solution)/shard_map/while/body/eval_jaxpr/ppermute | solution.py:9
  845.8 12.5 %collective-permute-done = bf16[128,2048]{1,0:T(8,128)(2,1)S(1)} collective-permute-done((bf16[128,2048]{1,0:T(8,128)(2,1)S(1)}, bf16[128,2048]{1,0:T(8,128)(2,1)S(1)}, u32[]{:S(2)}, u32[]{:S(2)}) %collective-permute-start) | collective-permute-done | bytes 524320 | tf_op jit(solution)/shard_map/while/body/eval_jaxpr/ppermute | solution.py:9
  (1606 shorter events, 182.8 us)
Async XLA Ops:
  18.1 17.1 %collective-permute-start = (bf16[128,2048]{1,0:T(8,128)(2,1)S(1)}, bf16[128,2048]{1,0:T(8,128)(2,1)S(1)}, u32[]{:S(2)}, u32[]{:S(2)}) collective-permute-start(bf16[128,2048]{1,0:T(8,128)(2,1)S(1)} %get-tuple-element.530), channel_id=1, source_target_pairs={{0,8},{8,16},{16,24},{24,32},{32,40},{40,48},{48,56},{56,64},{64,7... | collective-permute-start | bytes 1572872 | tf_op jit(solution)/shard_map/while/body/eval_jaxpr/ppermute | solution.py:9
  37.0 5.3 copy-start.2
  37.1 5.3 copy-start.3
  37.1 5.3 copy-start.4
  49.4 16.2 %collective-permute-start = (bf16[128,2048]{1,0:T(8,128)(2,1)S(1)}, bf16[128,2048]{1,0:T(8,128)(2,1)S(1)}, u32[]{:S(2)}, u32[]{:S(2)}) collective-permute-start(bf16[128,2048]{1,0:T(8,128)(2,1)S(1)} %get-tuple-element.530), channel_id=1, source_target_pairs={{0,8},{8,16},{16,24},{24,32},{32,40},{40,48},{48,56},{56,64},{64,7... | collective-permute-start | bytes 1572872 | tf_op jit(solution)/shard_map/while/body/eval_jaxpr/ppermute | solution.py:9
  67.5 5.3 copy-start.2
  67.5 5.3 copy-start.3
  67.5 5.3 copy-start.4
  79.8 15.3 %collective-permute-start = (bf16[128,2048]{1,0:T(8,128)(2,1)S(1)}, bf16[128,2048]{1,0:T(8,128)(2,1)S(1)}, u32[]{:S(2)}, u32[]{:S(2)}) collective-permute-start(bf16[128,2048]{1,0:T(8,128)(2,1)S(1)} %get-tuple-element.530), channel_id=1, source_target_pairs={{0,8},{8,16},{16,24},{24,32},{32,40},{40,48},{48,56},{56,64},{64,7... | collective-permute-start | bytes 1572872 | tf_op jit(solution)/shard_map/while/body/eval_jaxpr/ppermute | solution.py:9
  97.0 5.3 copy-start.2
  97.0 5.3 copy-start.3
  97.0 5.3 copy-start.4
  109.3 14.5 %collective-permute-start = (bf16[128,2048]{1,0:T(8,128)(2,1)S(1)}, bf16[128,2048]{1,0:T(8,128)(2,1)S(1)}, u32[]{:S(2)}, u32[]{:S(2)}) collective-permute-start(bf16[128,2048]{1,0:T(8,128)(2,1)S(1)} %get-tuple-element.530), channel_id=1, source_target_pairs={{0,8},{8,16},{16,24},{24,32},{32,40},{40,48},{48,56},{56,64},{64,7... | collective-permute-start | bytes 1572872 | tf_op jit(solution)/shard_map/while/body/eval_jaxpr/ppermute | solution.py:9
  125.7 5.3 copy-start.2
  125.7 5.3 copy-start.3
  125.7 5.3 copy-start.4
  138.0 13.6 %collective-permute-start = (bf16[128,2048]{1,0:T(8,128)(2,1)S(1)}, bf16[128,2048]{1,0:T(8,128)(2,1)S(1)}, u32[]{:S(2)}, u32[]{:S(2)}) collective-permute-start(bf16[128,2048]{1,0:T(8,128)(2,1)S(1)} %get-tuple-element.530), channel_id=1, source_target_pairs={{0,8},{8,16},{16,24},{24,32},{32,40},{40,48},{48,56},{56,64},{64,7... | collective-permute-start | bytes 1572872 | tf_op jit(solution)/shard_map/while/body/eval_jaxpr/ppermute | solution.py:9
  153.6 5.3 copy-start.2
  153.6 5.3 copy-start.3
  153.6 5.3 copy-start.4
  165.9 12.8 %collective-permute-start = (bf16[128,2048]{1,0:T(8,128)(2,1)S(1)}, bf16[128,2048]{1,0:T(8,128)(2,1)S(1)}, u32[]{:S(2)}, u32[]{:S(2)}) collective-permute-start(bf16[128,2048]{1,0:T(8,128)(2,1)S(1)} %get-tuple-element.530), channel_id=1, source_target_pairs={{0,8},{8,16},{16,24},{24,32},{32,40},{40,48},{48,56},{56,64},{64,7... | collective-permute-start | bytes 1572872 | tf_op jit(solution)/shard_map/while/body/eval_jaxpr/ppermute | solution.py:9
  180.6 5.3 copy-start.2
  180.6 5.3 copy-start.3
  180.6 5.3 copy-start.4
  192.9 12.6 %collective-permute-start = (bf16[128,2048]{1,0:T(8,128)(2,1)S(1)}, bf16[128,2048]{1,0:T(8,128)(2,1)S(1)}, u32[]{:S(2)}, u32[]{:S(2)}) collective-permute-start(bf16[128,2048]{1,0:T(8,128)(2,1)S(1)} %get-tuple-element.530), channel_id=1, source_target_pairs={{0,8},{8,16},{16,24},{24,32},{32,40},{40,48},{48,56},{56,64},{64,7... | collective-permute-start | bytes 1572872 | tf_op jit(solution)/shard_map/while/body/eval_jaxpr/ppermute | solution.py:9
  207.4 5.3 copy-start.2
  219.7 12.6 %collective-permute-start = (bf16[128,2048]{1,0:T(8,128)(2,1)S(1)}, bf16[128,2048]{1,0:T(8,128)(2,1)S(1)}, u32[]{:S(2)}, u32[]{:S(2)}) collective-permute-start(bf16[128,2048]{1,0:T(8,128)(2,1)S(1)} %get-tuple-element.530), channel_id=1, source_target_pairs={{0,8},{8,16},{16,24},{24,32},{32,40},{40,48},{48,56},{56,64},{64,7... | collective-permute-start | bytes 1572872 | tf_op jit(solution)/shard_map/while/body/eval_jaxpr/ppermute | solution.py:9
  234.2 5.3 copy-start.2
  234.2 5.3 copy-start.3
  246.5 12.6 %collective-permute-start = (bf16[128,2048]{1,0:T(8,128)(2,1)S(1)}, bf16[128,2048]{1,0:T(8,128)(2,1)S(1)}, u32[]{:S(2)}, u32[]{:S(2)}) collective-permute-start(bf16[128,2048]{1,0:T(8,128)(2,1)S(1)} %get-tuple-element.530), channel_id=1, source_target_pairs={{0,8},{8,16},{16,24},{24,32},{32,40},{40,48},{48,56},{56,64},{64,7... | collective-permute-start | bytes 1572872 | tf_op jit(solution)/shard_map/while/body/eval_jaxpr/ppermute | solution.py:9
  260.9 5.3 copy-start.2
  273.3 12.6 %collective-permute-start = (bf16[128,2048]{1,0:T(8,128)(2,1)S(1)}, bf16[128,2048]{1,0:T(8,128)(2,1)S(1)}, u32[]{:S(2)}, u32[]{:S(2)}) collective-permute-start(bf16[128,2048]{1,0:T(8,128)(2,1)S(1)} %get-tuple-element.530), channel_id=1, source_target_pairs={{0,8},{8,16},{16,24},{24,32},{32,40},{40,48},{48,56},{56,64},{64,7... | collective-permute-start | bytes 1572872 | tf_op jit(solution)/shard_map/while/body/eval_jaxpr/ppermute | solution.py:9
  287.7 5.3 copy-start.2
  287.7 5.3 copy-start.3
  300.1 12.6 %collective-permute-start = (bf16[128,2048]{1,0:T(8,128)(2,1)S(1)}, bf16[128,2048]{1,0:T(8,128)(2,1)S(1)}, u32[]{:S(2)}, u32[]{:S(2)}) collective-permute-start(bf16[128,2048]{1,0:T(8,128)(2,1)S(1)} %get-tuple-element.530), channel_id=1, source_target_pairs={{0,8},{8,16},{16,24},{24,32},{32,40},{40,48},{48,56},{56,64},{64,7... | collective-permute-start | bytes 1572872 | tf_op jit(solution)/shard_map/while/body/eval_jaxpr/ppermute | solution.py:9
  314.5 5.3 copy-start.2
  326.8 12.6 %collective-permute-start = (bf16[128,2048]{1,0:T(8,128)(2,1)S(1)}, bf16[128,2048]{1,0:T(8,128)(2,1)S(1)}, u32[]{:S(2)}, u32[]{:S(2)}) collective-permute-start(bf16[128,2048]{1,0:T(8,128)(2,1)S(1)} %get-tuple-element.530), channel_id=1, source_target_pairs={{0,8},{8,16},{16,24},{24,32},{32,40},{40,48},{48,56},{56,64},{64,7... | collective-permute-start | bytes 1572872 | tf_op jit(solution)/shard_map/while/body/eval_jaxpr/ppermute | solution.py:9
  341.3 5.3 copy-start.2
  341.3 5.3 copy-start.3
  353.6 12.6 %collective-permute-start = (bf16[128,2048]{1,0:T(8,128)(2,1)S(1)}, bf16[128,2048]{1,0:T(8,128)(2,1)S(1)}, u32[]{:S(2)}, u32[]{:S(2)}) collective-permute-start(bf16[128,2048]{1,0:T(8,128)(2,1)S(1)} %get-tuple-element.530), channel_id=1, source_target_pairs={{0,8},{8,16},{16,24},{24,32},{32,40},{40,48},{48,56},{56,64},{64,7... | collective-permute-start | bytes 1572872 | tf_op jit(solution)/shard_map/while/body/eval_jaxpr/ppermute | solution.py:9
  368.1 5.3 copy-start.2
  368.1 5.3 copy-start.3
  380.4 12.6 %collective-permute-start = (bf16[128,2048]{1,0:T(8,128)(2,1)S(1)}, bf16[128,2048]{1,0:T(8,128)(2,1)S(1)}, u32[]{:S(2)}, u32[]{:S(2)}) collective-permute-start(bf16[128,2048]{1,0:T(8,128)(2,1)S(1)} %get-tuple-element.530), channel_id=1, source_target_pairs={{0,8},{8,16},{16,24},{24,32},{32,40},{40,48},{48,56},{56,64},{64,7... | collective-permute-start | bytes 1572872 | tf_op jit(solution)/shard_map/while/body/eval_jaxpr/ppermute | solution.py:9
  394.9 5.3 copy-start.2
  407.2 12.6 %collective-permute-start = (bf16[128,2048]{1,0:T(8,128)(2,1)S(1)}, bf16[128,2048]{1,0:T(8,128)(2,1)S(1)}, u32[]{:S(2)}, u32[]{:S(2)}) collective-permute-start(bf16[128,2048]{1,0:T(8,128)(2,1)S(1)} %get-tuple-element.530), channel_id=1, source_target_pairs={{0,8},{8,16},{16,24},{24,32},{32,40},{40,48},{48,56},{56,64},{64,7... | collective-permute-start | bytes 1572872 | tf_op jit(solution)/shard_map/while/body/eval_jaxpr/ppermute | solution.py:9
  421.7 5.3 copy-start.2
  421.7 5.3 copy-start.3
  434.0 14.3 %collective-permute-start = (bf16[128,2048]{1,0:T(8,128)(2,1)S(1)}, bf16[128,2048]{1,0:T(8,128)(2,1)S(1)}, u32[]{:S(2)}, u32[]{:S(2)}) collective-permute-start(bf16[128,2048]{1,0:T(8,128)(2,1)S(1)} %get-tuple-element.530), channel_id=1, source_target_pairs={{0,8},{8,16},{16,24},{24,32},{32,40},{40,48},{48,56},{56,64},{64,7... | collective-permute-start | bytes 1572872 | tf_op jit(solution)/shard_map/while/body/eval_jaxpr/ppermute | solution.py:9
  448.4 23.1 %collective-permute-start = (bf16[128,2048]{1,0:T(8,128)(2,1)S(1)}, bf16[128,2048]{1,0:T(8,128)(2,1)S(1)}, u32[]{:S(2)}, u32[]{:S(2)}) collective-permute-start(bf16[128,2048]{1,0:T(8,128)(2,1)S(1)} %get-tuple-element.530), channel_id=1, source_target_pairs={{0,8},{8,16},{16,24},{24,32},{32,40},{40,48},{48,56},{56,64},{64,7... | collective-permute-start | bytes 1572872 | tf_op jit(solution)/shard_map/while/body/eval_jaxpr/ppermute | solution.py:9
  471.6 27.0 %collective-permute-start = (bf16[128,2048]{1,0:T(8,128)(2,1)S(1)}, bf16[128,2048]{1,0:T(8,128)(2,1)S(1)}, u32[]{:S(2)}, u32[]{:S(2)}) collective-permute-start(bf16[128,2048]{1,0:T(8,128)(2,1)S(1)} %get-tuple-element.530), channel_id=1, source_target_pairs={{0,8},{8,16},{16,24},{24,32},{32,40},{40,48},{48,56},{56,64},{64,7... | collective-permute-start | bytes 1572872 | tf_op jit(solution)/shard_map/while/body/eval_jaxpr/ppermute | solution.py:9
  498.7 28.2 %collective-permute-start = (bf16[128,2048]{1,0:T(8,128)(2,1)S(1)}, bf16[128,2048]{1,0:T(8,128)(2,1)S(1)}, u32[]{:S(2)}, u32[]{:S(2)}) collective-permute-start(bf16[128,2048]{1,0:T(8,128)(2,1)S(1)} %get-tuple-element.530), channel_id=1, source_target_pairs={{0,8},{8,16},{16,24},{24,32},{32,40},{40,48},{48,56},{56,64},{64,7... | collective-permute-start | bytes 1572872 | tf_op jit(solution)/shard_map/while/body/eval_jaxpr/ppermute | solution.py:9
  527.0 29.2 %collective-permute-start = (bf16[128,2048]{1,0:T(8,128)(2,1)S(1)}, bf16[128,2048]{1,0:T(8,128)(2,1)S(1)}, u32[]{:S(2)}, u32[]{:S(2)}) collective-permute-start(bf16[128,2048]{1,0:T(8,128)(2,1)S(1)} %get-tuple-element.530), channel_id=1, source_target_pairs={{0,8},{8,16},{16,24},{24,32},{32,40},{40,48},{48,56},{56,64},{64,7... | collective-permute-start | bytes 1572872 | tf_op jit(solution)/shard_map/while/body/eval_jaxpr/ppermute | solution.py:9
  556.3 27.8 %collective-permute-start = (bf16[128,2048]{1,0:T(8,128)(2,1)S(1)}, bf16[128,2048]{1,0:T(8,128)(2,1)S(1)}, u32[]{:S(2)}, u32[]{:S(2)}) collective-permute-start(bf16[128,2048]{1,0:T(8,128)(2,1)S(1)} %get-tuple-element.530), channel_id=1, source_target_pairs={{0,8},{8,16},{16,24},{24,32},{32,40},{40,48},{48,56},{56,64},{64,7... | collective-permute-start | bytes 1572872 | tf_op jit(solution)/shard_map/while/body/eval_jaxpr/ppermute | solution.py:9
  584.2 27.0 %collective-permute-start = (bf16[128,2048]{1,0:T(8,128)(2,1)S(1)}, bf16[128,2048]{1,0:T(8,128)(2,1)S(1)}, u32[]{:S(2)}, u32[]{:S(2)}) collective-permute-start(bf16[128,2048]{1,0:T(8,128)(2,1)S(1)} %get-tuple-element.530), channel_id=1, source_target_pairs={{0,8},{8,16},{16,24},{24,32},{32,40},{40,48},{48,56},{56,64},{64,7... | collective-permute-start | bytes 1572872 | tf_op jit(solution)/shard_map/while/body/eval_jaxpr/ppermute | solution.py:9
  611.2 26.1 %collective-permute-start = (bf16[128,2048]{1,0:T(8,128)(2,1)S(1)}, bf16[128,2048]{1,0:T(8,128)(2,1)S(1)}, u32[]{:S(2)}, u32[]{:S(2)}) collective-permute-start(bf16[128,2048]{1,0:T(8,128)(2,1)S(1)} %get-tuple-element.530), channel_id=1, source_target_pairs={{0,8},{8,16},{16,24},{24,32},{32,40},{40,48},{48,56},{56,64},{64,7... | collective-permute-start | bytes 1572872 | tf_op jit(solution)/shard_map/while/body/eval_jaxpr/ppermute | solution.py:9
  637.4 25.2 %collective-permute-start = (bf16[128,2048]{1,0:T(8,128)(2,1)S(1)}, bf16[128,2048]{1,0:T(8,128)(2,1)S(1)}, u32[]{:S(2)}, u32[]{:S(2)}) collective-permute-start(bf16[128,2048]{1,0:T(8,128)(2,1)S(1)} %get-tuple-element.530), channel_id=1, source_target_pairs={{0,8},{8,16},{16,24},{24,32},{32,40},{40,48},{48,56},{56,64},{64,7... | collective-permute-start | bytes 1572872 | tf_op jit(solution)/shard_map/while/body/eval_jaxpr/ppermute | solution.py:9
  662.7 24.4 %collective-permute-start = (bf16[128,2048]{1,0:T(8,128)(2,1)S(1)}, bf16[128,2048]{1,0:T(8,128)(2,1)S(1)}, u32[]{:S(2)}, u32[]{:S(2)}) collective-permute-start(bf16[128,2048]{1,0:T(8,128)(2,1)S(1)} %get-tuple-element.530), channel_id=1, source_target_pairs={{0,8},{8,16},{16,24},{24,32},{32,40},{40,48},{48,56},{56,64},{64,7... | collective-permute-start | bytes 1572872 | tf_op jit(solution)/shard_map/while/body/eval_jaxpr/ppermute | solution.py:9
  687.2 27.6 %collective-permute-start = (bf16[128,2048]{1,0:T(8,128)(2,1)S(1)}, bf16[128,2048]{1,0:T(8,128)(2,1)S(1)}, u32[]{:S(2)}, u32[]{:S(2)}) collective-permute-start(bf16[128,2048]{1,0:T(8,128)(2,1)S(1)} %get-tuple-element.530), channel_id=1, source_target_pairs={{0,8},{8,16},{16,24},{24,32},{32,40},{40,48},{48,56},{56,64},{64,7... | collective-permute-start | bytes 1572872 | tf_op jit(solution)/shard_map/while/body/eval_jaxpr/ppermute | solution.py:9
  714.8 25.5 %collective-permute-start = (bf16[128,2048]{1,0:T(8,128)(2,1)S(1)}, bf16[128,2048]{1,0:T(8,128)(2,1)S(1)}, u32[]{:S(2)}, u32[]{:S(2)}) collective-permute-start(bf16[128,2048]{1,0:T(8,128)(2,1)S(1)} %get-tuple-element.530), channel_id=1, source_target_pairs={{0,8},{8,16},{16,24},{24,32},{32,40},{40,48},{48,56},{56,64},{64,7... | collective-permute-start | bytes 1572872 | tf_op jit(solution)/shard_map/while/body/eval_jaxpr/ppermute | solution.py:9
  740.4 24.6 %collective-permute-start = (bf16[128,2048]{1,0:T(8,128)(2,1)S(1)}, bf16[128,2048]{1,0:T(8,128)(2,1)S(1)}, u32[]{:S(2)}, u32[]{:S(2)}) collective-permute-start(bf16[128,2048]{1,0:T(8,128)(2,1)S(1)} %get-tuple-element.530), channel_id=1, source_target_pairs={{0,8},{8,16},{16,24},{24,32},{32,40},{40,48},{48,56},{56,64},{64,7... | collective-permute-start | bytes 1572872 | tf_op jit(solution)/shard_map/while/body/eval_jaxpr/ppermute | solution.py:9
  765.0 24.5 %collective-permute-start = (bf16[128,2048]{1,0:T(8,128)(2,1)S(1)}, bf16[128,2048]{1,0:T(8,128)(2,1)S(1)}, u32[]{:S(2)}, u32[]{:S(2)}) collective-permute-start(bf16[128,2048]{1,0:T(8,128)(2,1)S(1)} %get-tuple-element.530), channel_id=1, source_target_pairs={{0,8},{8,16},{16,24},{24,32},{32,40},{40,48},{48,56},{56,64},{64,7... | collective-permute-start | bytes 1572872 | tf_op jit(solution)/shard_map/while/body/eval_jaxpr/ppermute | solution.py:9
  789.6 26.7 %collective-permute-start = (bf16[128,2048]{1,0:T(8,128)(2,1)S(1)}, bf16[128,2048]{1,0:T(8,128)(2,1)S(1)}, u32[]{:S(2)}, u32[]{:S(2)}) collective-permute-start(bf16[128,2048]{1,0:T(8,128)(2,1)S(1)} %get-tuple-element.530), channel_id=1, source_target_pairs={{0,8},{8,16},{16,24},{24,32},{32,40},{40,48},{48,56},{56,64},{64,7... | collective-permute-start | bytes 1572872 | tf_op jit(solution)/shard_map/while/body/eval_jaxpr/ppermute | solution.py:9
  816.4 29.2 %collective-permute-start = (bf16[128,2048]{1,0:T(8,128)(2,1)S(1)}, bf16[128,2048]{1,0:T(8,128)(2,1)S(1)}, u32[]{:S(2)}, u32[]{:S(2)}) collective-permute-start(bf16[128,2048]{1,0:T(8,128)(2,1)S(1)} %get-tuple-element.530), channel_id=1, source_target_pairs={{0,8},{8,16},{16,24},{24,32},{32,40},{40,48},{48,56},{56,64},{64,7... | collective-permute-start | bytes 1572872 | tf_op jit(solution)/shard_map/while/body/eval_jaxpr/ppermute | solution.py:9
  845.7 12.6 %collective-permute-start = (bf16[128,2048]{1,0:T(8,128)(2,1)S(1)}, bf16[128,2048]{1,0:T(8,128)(2,1)S(1)}, u32[]{:S(2)}, u32[]{:S(2)}) collective-permute-start(bf16[128,2048]{1,0:T(8,128)(2,1)S(1)} %get-tuple-element.530), channel_id=1, source_target_pairs={{0,8},{8,16},{16,24},{24,32},{32,40},{40,48},{48,56},{56,64},{64,7... | collective-permute-start | bytes 1572872 | tf_op jit(solution)/shard_map/while/body/eval_jaxpr/ppermute | solution.py:9
  (33 other events, 162.2 us)
where the time goes:
time: 862 us; the launch traced here: 859 us
  waiting for transfers between devices  614 us (71%)
  matrix products  122 us (14%)
  local copies, waits for them, and re-layouts  62 us (7%)
  other arithmetic  39.8 us (5%)
  starting transfers between devices  11.4 us (1%)
  loops' own time  10.4 us (1%)
    ppermute x32, waiting for transfers between devices, from_behind(): lax.ppermute(value, axis, [(i, (i + by) % devices) for i in range(devices)])  614 us
    dot_general x16, matrix products, one_layer(): jnp.dot(states, output_projected, preferred_element_type=jnp.float32)  49.1 us
    dot_general x16, matrix products, one_layer(): jnp.dot(normed, input_projected, preferred_element_type=jnp.float32)  47.6 us
    slice x624, local copies, waits for them, and re-layouts, one_layer(): lax.associative_scan(combine_pair, (decay, update), axis=0)[1]  29.5 us
    dot_general x16, matrix products, one_layer(): jnp.einsum('ngi,gij->ngj', grouped, injection_weight, preferred_element_t...  20 us
  transfers between devices with their start and end apart: 32, of which 32 were waited for; matrix products, arithmetic and copies ran while one was open for 0% of the time, Pallas kernels for 0%

commit v1 on v0

v1 whole, which is shorter than its diff:
```python
import functools

import jax
import jax.numpy as jnp
from jax import lax
from jax.experimental import pallas as pl
from jax.experimental.pallas import tpu as pltpu
from jax.sharding import PartitionSpec as P

PLANE = 4
SUB = 8
PARTS = 16
MESH = pl.DeviceIdType.MESH


def shifted(blocks, masked, delay):
    steps = blocks.shape[0]
    if delay == 0:
        return blocks
    return jnp.concatenate([masked[3 - delay :], blocks[: steps - delay]], axis=0)


def layer(hidden, win, wout, gates, vec, spike, normed, states):
    length, width = hidden.shape
    inner = win.shape[1]
    steps = length // SUB
    top = lax.broadcasted_iota(jnp.int32, (SUB, 128), 0)

    total = jnp.zeros((length, 128), jnp.float32)
    for n in range(width // 128):
        part = hidden[:, n * 128 : (n + 1) * 128].astype(jnp.float32)
        total = total + part * part
    scale = lax.rsqrt(jnp.sum(total, axis=1, keepdims=True) * (1.0 / width) + 1e-6)
    for n in range(width // 256):
        cols = slice(n * 256, (n + 1) * 256)
        row, start = divmod(n * 256, inner)
        gain = vec[row : row + 1, start : start + 256]
        normed[:, cols] = (hidden[:, cols].astype(jnp.float32) * scale * gain).astype(jnp.bfloat16)

    spikes = spike[...].reshape(steps, SUB, 128)
    for n in range(inner // 256):
        mixed2 = jnp.dot(
            normed[...], win[:, n * 256 : (n + 1) * 256], preferred_element_type=jnp.float32
        )
        for half in range(2):
            block = 2 * n + half
            cols = slice(block * 128, (block + 1) * 128)
            mixed = mixed2[:, half * 128 : (half + 1) * 128]
            mixed = mixed.astype(jnp.bfloat16).astype(jnp.float32).reshape(steps, SUB, 128)
            before = [
                jnp.where(top == 0, 0.0, pltpu.roll(mixed[steps - 3 + d], 1, 0))[None]
                for d in range(3)
            ]
            before = jnp.concatenate(before, axis=0)
            conv = vec[6:7, cols][None] + sum(
                shifted(mixed, before, 3 - k) * vec[2 + k : 3 + k, cols][None] for k in range(4)
            )
            conv = conv.reshape(length, 128).astype(jnp.bfloat16)
            pre = jnp.dot(
                conv, gates[block * 128 : (block + 1) * 128, :], preferred_element_type=jnp.float32
            )
            recall = 0.5 * jnp.tanh(0.5 * (pre[:, :128] + vec[7:8, cols])) + 0.5
            inject = 0.5 * jnp.tanh(0.5 * (pre[:, 128:] + vec[8:9, cols])) + 0.5
            log_decay = recall.reshape(steps, SUB, 128) * vec[9:10, cols][None] + spikes
            decay = jnp.exp(log_decay)
            update = (
                jnp.sqrt(jnp.maximum(1.0 - decay * decay, 0.0))
                * inject.reshape(steps, SUB, 128)
                * conv.astype(jnp.float32).reshape(steps, SUB, 128)
            )
            sums = [update[0]]
            factors = [decay[0]]
            for t in range(1, steps):
                sums.append(decay[t] * sums[-1] + update[t])
                factors.append(decay[t] * factors[-1])
            last, factor = sums[-1], factors[-1]
            for hop in (1, 2, 4):
                last = last + factor * jnp.where(top < hop, 0.0, pltpu.roll(last, hop, 0))
                if hop < 4:
                    factor = factor * jnp.where(top < hop, 1.0, pltpu.roll(factor, hop, 0))
            carry = jnp.where(top == 0, 0.0, pltpu.roll(last, 1, 0))
            done = jnp.concatenate(
                [(sums[t] + factors[t] * carry)[None] for t in range(steps)], axis=0
            )
            states[:, cols] = done.reshape(length, 128).astype(jnp.bfloat16)

    for n in range(width // 256):
        cols = slice(n * 256, (n + 1) * 256)
        projected = jnp.dot(states[...], wout[:, cols], preferred_element_type=jnp.float32)
        hidden[:, cols] = (hidden[:, cols].astype(jnp.float32) + projected).astype(jnp.bfloat16)


def kernel(
    planes, columns,
    tok, win, wout, gates, vec, spike, out,
    win_all, wout_all, gates_all, vec_all, spike_all, act, normed, states,
    y_recv, x_recv, d_recv, y_send, x_send, d_send, own_sem,
    small_recv, small_send, act_recv, act_send, tok_sem, out_recv,
):
    position = lax.axis_index("pp")
    x = lax.axis_index("fs")
    core = lax.axis_index("tp")
    z = position // PLANE
    y = lax.rem(position, PLANE)
    parity = lax.rem(x, 2)

    def at_y(by):
        return z * PLANE + lax.rem(y + by, PLANE)

    def plane_slot(by):
        return lax.rem(y + by, PLANE)

    up, down, across = {"pp": at_y(1)}, {"pp": at_y(3)}, {"pp": at_y(2)}
    right, left = {"fs": lax.rem(x + 1, columns)}, {"fs": lax.rem(x + columns - 1, columns)}
    sibling = {"tp": 1 - core}
    z_peers = [{"pp": lax.rem(z + by, planes) * PLANE + y} for by in range(1, planes)]

    barrier = pltpu.get_barrier_semaphore()
    peers = [up, down, across, right, left, sibling] + z_peers
    for peer in peers:
        pl.semaphore_signal(barrier, inc=1, device_id=peer, device_id_type=MESH)
    pl.semaphore_wait(barrier, len(peers))

    sources = (win, wout, gates)
    gathered = (win_all, wout_all, gates_all)
    heights = tuple(ref.shape[0] // PARTS for ref in sources)

    def piece_rows(a, piece):
        return pl.ds(pl.multiple_of(piece * heights[a], heights[a]), heights[a])

    def send(a, src, slot, piece, send_sem, recv_sem, to):
        pltpu.make_async_remote_copy(
            src_ref=src,
            dst_ref=gathered[a].at[slot, piece_rows(a, piece)],
            send_sem=send_sem,
            recv_sem=recv_sem,
            device_id=to,
            device_id_type=MESH,
        ).start()

    def await_bytes(ref, sem):
        pltpu.make_async_copy(ref, ref, sem).wait()

    mine = 8 * parity + 4 * core
    other = 8 * (1 - parity) + 4 * core

    for unit in range(4):
        for a in range(3):
            j = unit
            send(a, sources[a].at[piece_rows(a, mine + j)], y, mine + j,
                 y_send.at[0, a], y_recv.at[0, unit, a], up)
            j = (unit + 2) % 4
            send(a, sources[a].at[piece_rows(a, mine + j)], y, mine + j,
                 y_send.at[1, a], y_recv.at[1, unit, a], down)
    smalls = ((vec, vec_all), (spike, spike_all))
    for n, (src, dst) in enumerate(smalls):
        for by in range(1, 4):
            pltpu.make_async_remote_copy(
                src_ref=src, dst_ref=dst.at[y], send_sem=small_send.at[n, by - 1],
                recv_sem=small_recv.at[n, by - 1],
                device_id={"pp": at_y(by)}, device_id_type=MESH,
            ).start()

    @pl.when(z != 0)
    def _():
        pltpu.make_async_remote_copy(
            src_ref=tok, dst_ref=act.at[z], send_sem=tok_sem, recv_sem=act_recv.at[z],
            device_id={"pp": y}, device_id_type=MESH,
        ).start()

    @pl.when(z == 0)
    def _():
        pltpu.make_async_copy(tok, act.at[0], act_recv.at[0]).start()

    own = [pltpu.make_async_copy(sources[a], gathered[a].at[y], own_sem.at[a]) for a in range(3)]
    own += [pltpu.make_async_copy(src, dst.at[y], own_sem.at[3 + n])
            for n, (src, dst) in enumerate(smalls)]
    for copy in own:
        copy.start()

    def arrivals(unit):
        from_below = (plane_slot(3), unit) if unit < 4 else (plane_slot(2), unit - 4)
        from_above = (plane_slot(1), (unit + 2) % 4) if unit < 4 else (plane_slot(2), unit - 2)
        return from_below, from_above

    def relay_x(unit, a):
        for side, (slot, j) in enumerate(x_units[unit]):
            ref = gathered[a].at[slot, piece_rows(a, other + j)]
            await_bytes(ref, x_recv.at[side, unit, a])
            send(a, ref, slot, other + j, d_send.at[a], d_recv.at[a], sibling)

    x_units = []
    for unit in range(6):
        below, above = arrivals(unit)
        x_units.append((below, above) if below[1] < 2 else (above, below))

    for unit in range(7):
        for a in range(3):
            if unit < 6:
                below, above = arrivals(unit)
                for side, (slot, j) in enumerate((below, above)):
                    ref = gathered[a].at[slot, piece_rows(a, mine + j)]
                    await_bytes(ref, y_recv.at[side, unit, a])
                    if unit < 2:
                        send(a, ref, slot, mine + j, y_send.at[side, a],
                             y_recv.at[side, 4 + unit, a], up if side == 0 else down)
                    x_side = 0 if j < 2 else 1
                    send(a, ref, slot, mine + j, x_send.at[x_side, a],
                         x_recv.at[x_side, unit, a], left if x_side == 0 else right)
                    send(a, ref, slot, mine + j, d_send.at[a], d_recv.at[a], sibling)
            if unit > 0:
                relay_x(unit - 1, a)

    for copy in own:
        copy.wait()
    for n, (src, dst) in enumerate(smalls):
        for by in range(1, 4):
            await_bytes(dst.at[plane_slot(4 - by)], small_recv.at[n, by - 1])
    for a in range(3):
        whole = gathered[a].at[pl.ds(0, 2), pl.ds(0, 12 * heights[a])]
        await_bytes(whole, d_recv.at[a])

    def micro(i, token):
        await_bytes(act.at[i], act_recv.at[i])

        def one(s, token):
            layer(act.at[i], win_all.at[s], wout_all.at[s], gates_all.at[s],
                  vec_all.at[s], spike_all.at[s], normed, states)
            return token

        lax.fori_loop(0, PLANE, one, 0)

        @pl.when(z < planes - 1)
        def _():
            pltpu.make_async_remote_copy(
                src_ref=act.at[i], dst_ref=act.at[i], send_sem=act_send.at[i],
                recv_sem=act_recv.at[i],
                device_id={"pp": lax.rem(z + 1, planes) * PLANE + y}, device_id_type=MESH,
            ).start()

        @pl.when((z == planes - 1) & (i < planes - 1))
        def _():
            pltpu.make_async_remote_copy(
                src_ref=act.at[i], dst_ref=out, send_sem=act_send.at[i],
                recv_sem=out_recv,
                device_id={"pp": i * PLANE + y}, device_id_type=MESH,
            ).start()

        @pl.when((z == planes - 1) & (i == planes - 1))
        def _():
            pltpu.make_async_copy(act.at[i], out, out_recv).start()

        return token

    lax.fori_loop(0, planes, micro, 0)

    await_bytes(out, out_recv)
    for i in range(planes):
        if i < planes - 1:
            await_bytes(act.at[i], act_send.at[i])
        else:
            @pl.when(z < planes - 1)
            def _():
                await_bytes(act.at[i], act_send.at[i])

    @pl.when(z != 0)
    def _():
        await_bytes(tok, tok_sem)

    for n, (src, dst) in enumerate(smalls):
        for by in range(1, 4):
            await_bytes(src, small_send.at[n, by - 1])
    for a in range(3):
        for side in range(2):
            half = gathered[a].at[0, pl.ds(0, 6 * heights[a])]
            await_bytes(half, y_send.at[side, a])
            await_bytes(half, x_send.at[side, a])
        whole = gathered[a].at[pl.ds(0, 2), pl.ds(0, 12 * heights[a])]
        await_bytes(whole, d_send.at[a])


def by_lane(rows):
    length = rows.shape[0]
    return rows.reshape(SUB, length // SUB, -1).swapaxes(0, 1).reshape(length, -1)


def by_time(rows):
    length = rows.shape[0]
    return rows.reshape(length // SUB, SUB, -1).swapaxes(0, 1).reshape(length, -1)


def local(
    tokens,
    layer_norm_scale,
    input_weight,
    filter_weight,
    filter_bias,
    recur_gate_weight,
    recur_gate_bias,
    input_gate_weight,
    input_gate_bias,
    decay_setting,
    spike_log_decay,
    output_weight,
):
    planes = lax.axis_size("pp") // PLANE
    columns = lax.axis_size("fs")
    length, width = tokens.shape[2:]
    inner = input_weight.shape[2]
    tok = by_lane(tokens[0, 0])
    gates = jnp.concatenate([recur_gate_weight[0], input_gate_weight[0]], axis=2).reshape(inner, 256)
    vec = jnp.concatenate(
        [
            layer_norm_scale[0].reshape(-1, inner),
            filter_weight[0],
            filter_bias,
            recur_gate_bias,
            input_gate_bias,
            -8.0 * jax.nn.softplus(-decay_setting),
            jnp.zeros((16 - 8 - width // inner, inner), jnp.float32),
        ],
        axis=0,
    )
    spike = jnp.broadcast_to(by_lane(spike_log_decay[0][:, None]), (length, 128))
    dma = pltpu.SemaphoreType.DMA
    hbm = pl.BlockSpec(memory_space=pl.ANY)
    finished = pl.pallas_call(
        functools.partial(kernel, planes, columns),
        out_shape=jax.ShapeDtypeStruct((length, width), jnp.bfloat16),
        in_specs=[hbm] * 6,
        out_specs=hbm,
        scratch_shapes=[
            pltpu.VMEM((PLANE, width, inner), jnp.bfloat16),
            pltpu.VMEM((PLANE, inner, width), jnp.bfloat16),
            pltpu.VMEM((PLANE, inner, 256), jnp.bfloat16),
            pltpu.VMEM((PLANE, 16, inner), jnp.float32),
            pltpu.VMEM((PLANE, length, 128), jnp.float32),
            pltpu.VMEM((planes, length, width), jnp.bfloat16),
            pltpu.VMEM((length, width), jnp.bfloat16),
            pltpu.VMEM((length, inner), jnp.bfloat16),
            dma((2, 6, 3)),
            dma((2, 6, 3)),
            dma((3,)),
            dma((2, 3)),
            dma((2, 3)),
            dma((3,)),
            dma((5,)),
            dma((2, 3)),
            dma((2, 3)),
            dma((planes,)),
            dma((planes,)),
            dma,
            dma,
        ],
        compiler_params=pltpu.CompilerParams(
            collective_id=0, has_side_effects=True, vmem_limit_bytes=60 * 1024 * 1024
        ),
    )(tok, input_weight[0], output_weight[0], gates, vec, spike)
    return by_time(finished)[None, None]


def solution(mesh):
    placed = (
        P("pp", ("fs", "tp"), None, None),
        P("pp", None),
        P("pp", None, None),
        P("pp", None, None),
        P("pp", None),
        P("pp", None, None, None),
        P("pp", None),
        P("pp", None, None, None),
        P("pp", None),
        P("pp", None),
        P("pp", None),
        P("pp", None, None),
    )
    return jax.shard_map(
        local,
        mesh=mesh,
        in_specs=placed,
        out_specs=P("pp", ("fs", "tp"), None, None),
        check_vma=False,
    )
```

time: 862 us -> 227 us (0.26)
  the two profiles are of different devices: /device:TPU:4 before, /device:TPU:97 now
where the time goes in v1:
time: 227 us; the launch traced here: 225 us
  Pallas kernels  211 us (93%)
  local copies, waits for them, and re-layouts  8.4 us (4%)
  other arithmetic  5.27 us (2%)
    pallas_call x1, Pallas kernels, local(): pl.pallas_call(functools.partial(kernel, planes, columns), out_shape=jax....  211 us

profile of v1, /device:TPU:97, one launch (start us, length us, event | category | flops | bytes accessed | tf_op | source)
XLA Modules:
  0.0 224.6 jit_solution(10593489230305411137)
XLA Ops:
  0.0 0.5 broadcast.6
  0.5 1.3 reduce.7
  1.8 0.1 reshape_broadcast_in_dim_squeeze.3
  1.9 0.1 copy.17
  2.0 0.1 broadcast_in_dim.11
  2.1 0.7 fusion
  2.8 1.4 reduce.6
  4.2 2.7 %concatenate.14.vec = f32[16,1024]{1,0:T(8,128)} concatenate(f32[2,1024]{1,0:T(2,128)S(1)} %reshape_squeeze.7, f32[4,1024]{1,0:T(4,128)} %bitcast.25, f32[1,1024]{1,0:T(1,128)} %param.16, f32[1,1024]{1,0:T(1,128)} %param.18, f32[1,1024]{1,0:T(1,128)} %param.20, f32[1,1024]{1,0:T(1,128)S(1)} %fusion, f32[6,1024]{1,0:T(8,128)S(1)} %broadcast_in_dim.10), dimensions={0} | concatenate | bytes 131072 | tf_op jit(solution)/shard_map/concatenate | solution.py:312
  6.9 0.7 broadcast_in_dim.12.spike
  7.6 2.1 copy.20
  9.7 1.9 pad_maximum_fusion.gates
  11.6 210.9 %shard_map.118 = bf16[128,2048]{1,0:T(8,128)(2,1)} custom-call(bf16[128,2048]{1,0:T(8,128)(2,1)} %bitcast.21, bf16[2048,1024]{1,0:T(8,128)(2,1)} %bitcast.18, bf16[1024,2048]{1,0:T(8,128)(2,1)} %bitcast.19, bf16[1024,256]{1,0:T(8,128)(2,1)} %pad_maximum_fusion.gates, f32[16,1024]{1,0:T(8,128)} %concatenate.14.vec, f32[128,128]{1,0:T(8,128)} %broadcast_in_dim.12.spike), custom_call_target="tpu_custom_call" | custom-call | tf_op jit(solution)/shard_map/pallas_call | solution.py:327
  222.5 2.1 copy.18
  (2 shorter events, 0.0 us)

commit v2 on v1

v2 whole, which is shorter than its diff:
```python
import functools

import jax
import jax.numpy as jnp
from jax import lax
from jax.experimental import pallas as pl
from jax.experimental.pallas import tpu as pltpu
from jax.sharding import PartitionSpec as P

PLANE = 4
SUB = 8
HALVES = 2
PARTS = 16
MESH = pl.DeviceIdType.MESH


def layer(hidden, win, wout, gates, vec, spike, tail, past, scaled, states):
    length, width = hidden.shape
    inner = win.shape[1]
    steps = length // SUB
    top = lax.broadcasted_iota(jnp.int32, (SUB, 128), 0)

    total = jnp.zeros((length, 128), jnp.float32)
    for n in range(width // 128):
        cols = slice(n * 128, (n + 1) * 128)
        row, start = divmod(n * 128, inner)
        part = hidden[:, cols].astype(jnp.float32)
        total = total + part * part
        scaled[:, cols] = (part * vec[row : row + 1, start : start + 128]).astype(jnp.bfloat16)
    scale = lax.rsqrt(jnp.sum(total, axis=1, keepdims=True) * (1.0 / width) + 1e-6)
    scale = jnp.broadcast_to(scale, (length, 128))
    spikes = spike[...].reshape(steps, SUB, 128)

    def project(n):
        return jnp.dot(
            scaled[...], win[:, n * 256 : (n + 1) * 256], preferred_element_type=jnp.float32
        )

    def recur(mixed, block):
        cols = slice(block * 128, (block + 1) * 128)
        mixed = (mixed * scale).astype(jnp.bfloat16).astype(jnp.float32).reshape(steps, SUB, 128)
        taps = [vec[2 + k : 3 + k, cols] for k in range(4)]
        bias = vec[6:7, cols]
        before = []
        for d in range(3):
            rows = slice(d * SUB, (d + 1) * SUB)
            rolled = pltpu.roll(mixed[steps - 3 + d], 1, 0)
            before.append(jnp.where(top == 0, tail[rows, cols], rolled))
            tail[rows, cols] = rolled
        line = before + [mixed[t] for t in range(steps)]
        conv = jnp.concatenate(
            [
                (bias + sum(line[t + k] * taps[k] for k in range(4)))[None]
                for t in range(steps)
            ],
            axis=0,
        )
        conv = conv.reshape(length, 128).astype(jnp.bfloat16)
        pre = jnp.dot(
            conv, gates[block], preferred_element_type=jnp.float32
        )
        recall = 0.5 * jnp.tanh(0.5 * (pre[:, :128] + vec[7:8, cols])) + 0.5
        inject = 0.5 * jnp.tanh(0.5 * (pre[:, 128:] + vec[8:9, cols])) + 0.5
        log_decay = recall.reshape(steps, SUB, 128) * vec[9:10, cols][None] + spikes
        decay = jnp.exp(log_decay)
        room = jnp.maximum(1.0 - decay * decay, 1e-30)
        update = (
            room * lax.rsqrt(room)
            * inject.reshape(steps, SUB, 128)
            * conv.astype(jnp.float32).reshape(steps, SUB, 128)
        )
        sums = [update[0]]
        factors = [decay[0]]
        for t in range(1, steps):
            sums.append(decay[t] * sums[-1] + update[t])
            factors.append(decay[t] * factors[-1])
        first = past[:, cols]
        factor = factors[-1]
        last = sums[-1] + jnp.where(top == 0, factor * first, 0.0)
        for hop in (1, 2, 4):
            last = last + factor * jnp.where(top < hop, 0.0, pltpu.roll(last, hop, 0))
            if hop < 4:
                factor = factor * jnp.where(top < hop, 1.0, pltpu.roll(factor, hop, 0))
        ahead = pltpu.roll(last, 1, 0)
        past[:, cols] = ahead
        carry = jnp.where(top == 0, first, ahead)
        done = jnp.concatenate(
            [(sums[t] + factors[t] * carry)[None] for t in range(steps)], axis=0
        )
        states[:, cols] = done.reshape(length, 128).astype(jnp.bfloat16)

    groups = inner // 256
    mixed = project(0)
    for n in range(groups):
        following = project(n + 1) if n + 1 < groups else None
        recur(mixed[:, :128], 2 * n)
        recur(mixed[:, 128:], 2 * n + 1)
        mixed = following

    for n in range(width // 256):
        cols = slice(n * 256, (n + 1) * 256)
        projected = jnp.dot(states[...], wout[:, cols], preferred_element_type=jnp.float32)
        hidden[:, cols] = (hidden[:, cols].astype(jnp.float32) + projected).astype(jnp.bfloat16)


def reorder(src, dst):
    length = src.shape[0]
    steps = length // SUB
    row = lax.broadcasted_iota(jnp.int32, (length, length), 0)
    col = lax.broadcasted_iota(jnp.int32, (length, length), 1)
    swap = jnp.where(col == lax.rem(row, SUB) * steps + lax.div(row, SUB), 1.0, 0.0)
    swap = swap.astype(jnp.bfloat16)
    for n in range(src.shape[1] // 256):
        cols = slice(n * 256, (n + 1) * 256)
        moved = jnp.dot(swap, src[:, cols], preferred_element_type=jnp.float32)
        dst[:, cols] = moved.astype(jnp.bfloat16)


def kernel(
    planes, columns,
    tok, gain, win, taps, conv_bias, recur_gate, recur_bias, input_gate, input_bias, setting,
    spikes, wout, out,
    win_all, wout_all, gates_all, vec_all, spike_all, raw, home, act, final, tails, pasts,
    scaled, states,
    y_recv, x_recv, d_recv, y_send, x_send, d_send, own_sem,
    small_recv, small_send, raw_sem, act_recv, act_send, home_sem, out_recv,
):
    position = lax.axis_index("pp")
    x = lax.axis_index("fs")
    core = lax.axis_index("tp")
    z = position // PLANE
    y = lax.rem(position, PLANE)
    parity = lax.rem(x, 2)
    length, width = raw.shape
    inner = win_all.shape[2]
    chunk = length // HALVES

    def at_y(by):
        return z * PLANE + lax.rem(y + by, PLANE)

    def plane_slot(by):
        return lax.rem(y + by, PLANE)

    def rows_of(half):
        return pl.ds(pl.multiple_of(half * chunk, chunk), chunk)

    up, down, across = {"pp": at_y(1)}, {"pp": at_y(3)}, {"pp": at_y(2)}
    right, left = {"fs": lax.rem(x + 1, columns)}, {"fs": lax.rem(x + columns - 1, columns)}
    sibling = {"tp": 1 - core}
    z_peers = [{"pp": lax.rem(z + by, planes) * PLANE + y} for by in range(1, planes)]

    own = [
        pltpu.make_async_copy(recur_gate.at[0], gates_all.at[y, :, :, pl.ds(0, 128)], own_sem.at[0]),
        pltpu.make_async_copy(input_gate.at[0], gates_all.at[y, :, :, pl.ds(128, 128)], own_sem.at[1]),
        pltpu.make_async_copy(win.at[0], win_all.at[y], own_sem.at[2]),
        pltpu.make_async_copy(wout.at[0], wout_all.at[y], own_sem.at[3]),
    ]
    for copy in own[:2]:
        copy.start()
    pltpu.make_async_copy(tok.at[0, 0], raw, raw_sem).start()

    barrier = pltpu.get_barrier_semaphore()
    peers = [up, down, across, right, left, sibling] + z_peers
    for peer in peers:
        pl.semaphore_signal(barrier, inc=1, device_id=peer, device_id_type=MESH)

    vec_all[y, 0:1] = gain[:, :inner]
    vec_all[y, 1:2] = gain[:, inner:]
    vec_all[y, 2:6] = taps[0]
    vec_all[y, 6:7] = conv_bias[...]
    vec_all[y, 7:8] = recur_bias[...]
    vec_all[y, 8:9] = input_bias[...]
    below = -setting[...]
    vec_all[y, 9:10] = -8.0 * (jnp.maximum(below, 0.0) + jnp.log1p(jnp.exp(-jnp.abs(below))))
    row = lax.broadcasted_iota(jnp.int32, (length, length), 0)
    col = lax.broadcasted_iota(jnp.int32, (length, length), 1)
    within = lax.rem(row, chunk)
    token = (row - within) + lax.rem(within, SUB) * (chunk // SUB) + lax.div(within, SUB)
    picked = jnp.sum(jnp.where(col == token, spikes[...], 0.0), axis=1, keepdims=True)
    spike_all[y] = jnp.broadcast_to(picked, (length, 128))

    pl.semaphore_wait(barrier, len(peers))

    gathered = (win_all, wout_all, gates_all)

    def piece(ref, a, index):
        if a == 2:
            return ref.at[index // 2, pl.ds(pl.multiple_of(lax.rem(index, 2) * 64, 64), 64)]
        height = win_all.shape[1] // PARTS if a == 0 else wout_all.shape[1] // PARTS
        return ref.at[pl.ds(pl.multiple_of(index * height, height), height)]

    def send(a, src, slot, index, send_sem, recv_sem, to):
        pltpu.make_async_remote_copy(
            src_ref=src,
            dst_ref=piece(gathered[a].at[slot], a, index),
            send_sem=send_sem,
            recv_sem=recv_sem,
            device_id=to,
            device_id_type=MESH,
        ).start()

    def await_bytes(ref, sem):
        pltpu.make_async_copy(ref, ref, sem).wait()

    def pieces_of(a, count):
        if a == 2:
            if count <= PARTS:
                return gates_all.at[0, pl.ds(0, count // 2)]
            return gates_all.at[pl.ds(0, 2), pl.ds(0, count // 4)]
        height = gathered[a].shape[1] // PARTS
        if count <= PARTS:
            return gathered[a].at[0, pl.ds(0, count * height)]
        return gathered[a].at[pl.ds(0, 2), pl.ds(0, count // 2 * height)]

    mine = 8 * parity + 4 * core
    other = 8 * (1 - parity) + 4 * core

    for unit in range(4):
        for a in range(3):
            if unit == 0 and a == 2:
                for copy in own[:2]:
                    copy.wait()
            source = (win.at[0], wout.at[0], gates_all.at[y])[a]
            j = unit
            send(a, piece(source, a, mine + j), y, mine + j,
                 y_send.at[0, a], y_recv.at[0, unit, a], up)
            j = (unit + 2) % 4
            send(a, piece(source, a, mine + j), y, mine + j,
                 y_send.at[1, a], y_recv.at[1, unit, a], down)
    smalls = (vec_all, spike_all)
    for n, ref in enumerate(smalls):
        for by in range(1, 4):
            pltpu.make_async_remote_copy(
                src_ref=ref.at[y], dst_ref=ref.at[y], send_sem=small_send.at[n, by - 1],
                recv_sem=small_recv.at[n, by - 1],
                device_id={"pp": at_y(by)}, device_id_type=MESH,
            ).start()
    for copy in own[2:]:
        copy.start()

    await_bytes(raw, raw_sem)
    for half in range(HALVES):
        rows = slice(half * chunk, (half + 1) * chunk)
        reorder(raw.at[rows], home.at[rows])

        @pl.when(z != 0)
        def _():
            pltpu.make_async_remote_copy(
                src_ref=home.at[rows], dst_ref=act.at[z, rows], send_sem=home_sem.at[half],
                recv_sem=act_recv.at[z, half],
                device_id={"pp": y}, device_id_type=MESH,
            ).start()

        @pl.when(z == 0)
        def _():
            pltpu.make_async_copy(home.at[rows], act.at[0, rows], act_recv.at[0, half]).start()

    def arrivals(unit):
        from_below = (plane_slot(3), unit) if unit < 4 else (plane_slot(2), unit - 4)
        from_above = (plane_slot(1), (unit + 2) % 4) if unit < 4 else (plane_slot(2), unit - 2)
        return from_below, from_above

    x_units = []
    for unit in range(6):
        below, above = arrivals(unit)
        x_units.append((below, above) if below[1] < 2 else (above, below))

    def relay_y(unit, a):
        for side, (slot, j) in enumerate(arrivals(unit)):
            ref = piece(gathered[a].at[slot], a, mine + j)
            await_bytes(ref, y_recv.at[side, unit, a])
            if unit < 2:
                send(a, ref, slot, mine + j, y_send.at[side, a],
                     y_recv.at[side, 4 + unit, a], up if side == 0 else down)
            x_side = 0 if j < 2 else 1
            send(a, ref, slot, mine + j, x_send.at[x_side, a],
                 x_recv.at[x_side, unit, a], left if x_side == 0 else right)
            send(a, ref, slot, mine + j, d_send.at[a], d_recv.at[a], sibling)

    def relay_x(unit, a):
        for side, (slot, j) in enumerate(x_units[unit]):
            ref = piece(gathered[a].at[slot], a, other + j)
            await_bytes(ref, x_recv.at[side, unit, a])
            send(a, ref, slot, other + j, d_send.at[a], d_recv.at[a], sibling)

    for unit in range(7):
        for a in range(3):
            if unit < 6:
                relay_y(unit, a)
            if unit > 0:
                relay_x(unit - 1, a)

    for copy in own[2:]:
        copy.wait()
    for n, ref in enumerate(smalls):
        for by in range(1, 4):
            await_bytes(ref.at[plane_slot(4 - by)], small_recv.at[n, by - 1])
    for a in range(3):
        await_bytes(pieces_of(a, 24), d_recv.at[a])

    def micro(step, token):
        i = step // HALVES
        half = lax.rem(step, HALVES)
        rows = rows_of(half)
        here = act.at[i, rows]
        await_bytes(here, act_recv.at[i, half])

        @pl.when(half == 0)
        def _():
            tails[...] = jnp.zeros_like(tails)
            pasts[...] = jnp.zeros_like(pasts)

        def one(s, token):
            layer(here, win_all.at[s], wout_all.at[s], gates_all.at[s], vec_all.at[s],
                  spike_all.at[s, rows], tails.at[s], pasts.at[s], scaled, states)
            return token

        lax.fori_loop(0, PLANE, one, 0)

        @pl.when(z < planes - 1)
        def _():
            pltpu.make_async_remote_copy(
                src_ref=here, dst_ref=here, send_sem=act_send.at[i, half],
                recv_sem=act_recv.at[i, half],
                device_id={"pp": lax.rem(z + 1, planes) * PLANE + y}, device_id_type=MESH,
            ).start()

        @pl.when(z == planes - 1)
        def _():
            reorder(here, final.at[i, rows])

            @pl.when(i < planes - 1)
            def _():
                pltpu.make_async_remote_copy(
                    src_ref=final.at[i, rows], dst_ref=out.at[0, 0, rows],
                    send_sem=act_send.at[i, half], recv_sem=out_recv.at[half],
                    device_id={"pp": i * PLANE + y}, device_id_type=MESH,
                ).start()

            @pl.when(i == planes - 1)
            def _():
                pltpu.make_async_copy(
                    final.at[i, rows], out.at[0, 0, rows], out_recv.at[half]
                ).start()

        return token

    lax.fori_loop(0, planes * HALVES, micro, 0)

    for half in range(HALVES):
        rows = slice(half * chunk, (half + 1) * chunk)
        await_bytes(out.at[0, 0, rows], out_recv.at[half])
        for i in range(planes):
            if i < planes - 1:
                await_bytes(act.at[i, rows], act_send.at[i, half])
            else:
                @pl.when(z < planes - 1)
                def _():
                    await_bytes(act.at[i, rows], act_send.at[i, half])

        @pl.when(z != 0)
        def _():
            await_bytes(home.at[rows], home_sem.at[half])

    for n, ref in enumerate(smalls):
        for by in range(1, 4):
            await_bytes(ref.at[y], small_send.at[n, by - 1])
    for a in range(3):
        for side in range(2):
            await_bytes(pieces_of(a, 6), y_send.at[side, a])
            await_bytes(pieces_of(a, 6), x_send.at[side, a])
        await_bytes(pieces_of(a, 24), d_send.at[a])


def local(
    tokens,
    layer_norm_scale,
    input_weight,
    filter_weight,
    filter_bias,
    recur_gate_weight,
    recur_gate_bias,
    input_gate_weight,
    input_gate_bias,
    decay_setting,
    spike_log_decay,
    output_weight,
):
    planes = lax.axis_size("pp") // PLANE
    columns = lax.axis_size("fs")
    length, width = tokens.shape[2:]
    inner = input_weight.shape[2]
    blocks = recur_gate_weight.shape[1]
    dma = pltpu.SemaphoreType.DMA
    hbm = pl.BlockSpec(memory_space=pl.ANY)
    near = pl.BlockSpec(memory_space=pltpu.VMEM)
    bf16, f32 = jnp.bfloat16, jnp.float32
    return pl.pallas_call(
        functools.partial(kernel, planes, columns),
        out_shape=jax.ShapeDtypeStruct(tokens.shape, bf16),
        in_specs=[hbm, near, hbm, near, near, hbm, near, hbm, near, near, near, hbm],
        out_specs=hbm,
        scratch_shapes=[
            pltpu.VMEM((PLANE, width, inner), bf16),
            pltpu.VMEM((PLANE, inner, width), bf16),
            pltpu.VMEM((PLANE, blocks, 128, 256), bf16),
            pltpu.VMEM((PLANE, 16, inner), f32),
            pltpu.VMEM((PLANE, length, 128), f32),
            pltpu.VMEM((length, width), bf16),
            pltpu.VMEM((length, width), bf16),
            pltpu.VMEM((planes, length, width), bf16),
            pltpu.VMEM((planes, length, width), bf16),
            pltpu.VMEM((PLANE, 3 * SUB, inner), f32),
            pltpu.VMEM((PLANE, SUB, inner), f32),
            pltpu.VMEM((length // HALVES, width), bf16),
            pltpu.VMEM((length // HALVES, inner), bf16),
            dma((2, 6, 3)),
            dma((2, 6, 3)),
            dma((3,)),
            dma((2, 3)),
            dma((2, 3)),
            dma((3,)),
            dma((4,)),
            dma((2, 3)),
            dma((2, 3)),
            dma,
            dma((planes, HALVES)),
            dma((planes, HALVES)),
            dma((HALVES,)),
            dma((HALVES,)),
        ],
        compiler_params=pltpu.CompilerParams(
            collective_id=0, has_side_effects=True, vmem_limit_bytes=60 * 1024 * 1024
        ),
    )(
        tokens,
        layer_norm_scale,
        input_weight,
        filter_weight,
        filter_bias,
        recur_gate_weight,
        recur_gate_bias,
        input_gate_weight,
        input_gate_bias,
        decay_setting,
        spike_log_decay,
        output_weight,
    )


def solution(mesh):
    placed = (
        P("pp", ("fs", "tp"), None, None),
        P("pp", None),
        P("pp", None, None),
        P("pp", None, None),
        P("pp", None),
        P("pp", None, None, None),
        P("pp", None),
        P("pp", None, None, None),
        P("pp", None),
        P("pp", None),
        P("pp", None),
        P("pp", None, None),
    )
    return jax.shard_map(
        local,
        mesh=mesh,
        in_specs=placed,
        out_specs=P("pp", ("fs", "tp"), None, None),
        check_vma=False,
    )
```

time: 227 us -> 211 us (0.930)
  local copies, waits for them, and re-layouts: 8.4 us -> 1.88 us
  other arithmetic: 5.27 us -> 0 us
  Pallas kernels: 211 us -> 208 us
    unnamed x2 -> x0, other arithmetic: 2.68 us -> none
    concatenate x1 -> x0, local copies, waits for them, and re-layouts: 2.67 us -> none  [local(): jnp.concatenate([layer_norm_scale[0].reshape(-1, inner), filter_weight[0]...]
    pallas_call x1, Pallas kernels: 211 us -> 208 us  [local(): pl.pallas_call(functools.partial(kernel, planes, columns), out_shape=jax....]
where the time goes in v2:
time: 211 us; the launch traced here: 210 us
  Pallas kernels  208 us (99%)
    pallas_call x1, Pallas kernels, local(): pl.pallas_call(functools.partial(kernel, planes, columns), out_shape=jax....  208 us

profile of v2, /device:TPU:97, one launch (start us, length us, event | category | flops | bytes accessed | tf_op | source)
XLA Modules:
  0.0 210.2 jit_solution(11196592181544079593)
XLA Ops:
  0.0 208.3 %shard_map.118 = bf16[1,1,128,2048]{3,2,1,0:T(8,128)(2,1)} custom-call(bf16[1,1,128,2048]{3,2,1,0:T(8,128)(2,1)} %tok.1, f32[1,2048]{1,0:T(1,128)} %gain.1, bf16[1,2048,1024]{2,1,0:T(8,128)(2,1)} %win.1, f32[1,4,1024]{2,1,0:T(4,128)} %taps.1, f32[1,1024]{1,0:T(1,128)} %conv_bias.1, bf16[1,8,128,128]{3,2,1,0:T(8,128)(2,1)} %recur_gate.1, ...), custom_call_target="tpu_custom_call" | custom-call | tf_op jit(solution)/shard_map/pallas_call | solution.py:398
  208.3 1.9 copy.14

commit v3 on v2

--- a/solution.py
+++ b/solution.py
@@ -9,17 +9,14 @@
 
 PLANE = 4
 SUB = 8
-HALVES = 2
+HALVES = 1
 PARTS = 16
 MESH = pl.DeviceIdType.MESH
 
 
-def layer(hidden, win, wout, gates, vec, spike, tail, past, scaled, states):
+def prepare(hidden, vec, scaled, power):
     length, width = hidden.shape
-    inner = win.shape[1]
-    steps = length // SUB
-    top = lax.broadcasted_iota(jnp.int32, (SUB, 128), 0)
-
+    inner = vec.shape[1]
     total = jnp.zeros((length, 128), jnp.float32)
     for n in range(width // 128):
         cols = slice(n * 128, (n + 1) * 128)
@@ -27,48 +24,50 @@
         part = hidden[:, cols].astype(jnp.float32)
         total = total + part * part
         scaled[:, cols] = (part * vec[row : row + 1, start : start + 128]).astype(jnp.bfloat16)
-    scale = lax.rsqrt(jnp.sum(total, axis=1, keepdims=True) * (1.0 / width) + 1e-6)
-    scale = jnp.broadcast_to(scale, (length, 128))
-    spikes = spike[...].reshape(steps, SUB, 128)
+    power[...] = total
+
+
+def layer(hidden, win, wout, gates, vec, following, spike, tail, past, scaled, power, states):
+    length, width = hidden.shape
+    inner = wout.shape[1]
+    steps = length // SUB
+    top = lax.broadcasted_iota(jnp.int32, (SUB, 128), 0)
 
     def project(n):
-        return jnp.dot(
-            scaled[...], win[:, n * 256 : (n + 1) * 256], preferred_element_type=jnp.float32
-        )
-
-    def recur(mixed, block):
+        weight = jnp.concatenate([win[2 * n], win[2 * n + 1]], axis=1)
+        return jnp.dot(scaled[...], weight, preferred_element_type=jnp.float32)
+
+    def conv_of(mixed, block):
         cols = slice(block * 128, (block + 1) * 128)
-        mixed = (mixed * scale).astype(jnp.bfloat16).astype(jnp.float32).reshape(steps, SUB, 128)
+        mixed = (mixed * scale).reshape(steps, SUB, 128)
         taps = [vec[2 + k : 3 + k, cols] for k in range(4)]
         bias = vec[6:7, cols]
-        before = []
+        line = []
         for d in range(3):
             rows = slice(d * SUB, (d + 1) * SUB)
             rolled = pltpu.roll(mixed[steps - 3 + d], 1, 0)
-            before.append(jnp.where(top == 0, tail[rows, cols], rolled))
+            line.append(jnp.where(top == 0, tail[rows, cols], rolled))
             tail[rows, cols] = rolled
-        line = before + [mixed[t] for t in range(steps)]
+        line += [mixed[t] for t in range(steps)]
         conv = jnp.concatenate(
             [
                 (bias + sum(line[t + k] * taps[k] for k in range(4)))[None]
                 for t in range(steps)
             ],
             axis=0,
-        )
-        conv = conv.reshape(length, 128).astype(jnp.bfloat16)
-        pre = jnp.dot(
-            conv, gates[block], preferred_element_type=jnp.float32
-        )
-        recall = 0.5 * jnp.tanh(0.5 * (pre[:, :128] + vec[7:8, cols])) + 0.5
-        inject = 0.5 * jnp.tanh(0.5 * (pre[:, 128:] + vec[8:9, cols])) + 0.5
-        log_decay = recall.reshape(steps, SUB, 128) * vec[9:10, cols][None] + spikes
-        decay = jnp.exp(log_decay)
+        ).reshape(length, 128)
+        weight = jnp.concatenate([gates[0, block], gates[1, block]], axis=1)
+        pre = jnp.dot(conv.astype(jnp.bfloat16), weight, preferred_element_type=jnp.float32)
+        return conv, pre
+
+    def recur(conv, pre, block):
+        cols = slice(block * 128, (block + 1) * 128)
+        rate = vec[9:10, cols]
+        recall = jnp.tanh(pre[:, :128] + vec[7:8, cols]).reshape(steps, SUB, 128)
+        inject = jnp.tanh(pre[:, 128:] + vec[8:9, cols]) + 1.0
+        decay = jnp.exp2(recall * rate[None] + (spikes + rate[None]))
         room = jnp.maximum(1.0 - decay * decay, 1e-30)
-        update = (
-            room * lax.rsqrt(room)
-            * inject.reshape(steps, SUB, 128)
-            * conv.astype(jnp.float32).reshape(steps, SUB, 128)
-        )
+        update = room * lax.rsqrt(room) * (inject * conv).reshape(steps, SUB, 128)
         sums = [update[0]]
         factors = [decay[0]]
         for t in range(1, steps):
@@ -91,23 +90,41 @@
 
     groups = inner // 256
     mixed = project(0)
+    scale = lax.rsqrt(jnp.sum(power[...], axis=1, keepdims=True) * (1.0 / width) + 1e-6)
+    scale = jnp.broadcast_to(scale, (length, 128))
+    spikes = spike[...].reshape(steps, SUB, 128)
     for n in range(groups):
-        following = project(n + 1) if n + 1 < groups else None
-        recur(mixed[:, :128], 2 * n)
-        recur(mixed[:, 128:], 2 * n + 1)
-        mixed = following
-
-    for n in range(width // 256):
-        cols = slice(n * 256, (n + 1) * 256)
-        projected = jnp.dot(states[...], wout[:, cols], preferred_element_type=jnp.float32)
-        hidden[:, cols] = (hidden[:, cols].astype(jnp.float32) + projected).astype(jnp.bfloat16)
-
-
-def reorder(src, dst):
+        later = project(n + 1) if n + 1 < groups else None
+        left = conv_of(mixed[:, :128], 2 * n)
+        right = conv_of(mixed[:, 128:], 2 * n + 1)
+        recur(*left, 2 * n)
+        recur(*right, 2 * n + 1)
+        mixed = later
+
+    total = jnp.zeros((length, 128), jnp.float32)
+    for m in range(width // 256):
+        weight = jnp.concatenate([wout[2 * m], wout[2 * m + 1]], axis=1)
+        projected = jnp.dot(states[...], weight, preferred_element_type=jnp.float32)
+        for half in range(2):
+            start = m * 256 + half * 128
+            cols = slice(start, start + 128)
+            part = hidden[:, cols].astype(jnp.float32) + projected[:, half * 128 : half * 128 + 128]
+            hidden[:, cols] = part.astype(jnp.bfloat16)
+            total = total + part * part
+            row, start = divmod(start, inner)
+            scaled[:, cols] = (part * following[row : row + 1, start : start + 128]).astype(
+                jnp.bfloat16
+            )
+    power[...] = total
+
+
+def reorder(src, dst, back):
     length = src.shape[0]
     steps = length // SUB
     row = lax.broadcasted_iota(jnp.int32, (length, length), 0)
     col = lax.broadcasted_iota(jnp.int32, (length, length), 1)
+    if back:
+        row, col = col, row
     swap = jnp.where(col == lax.rem(row, SUB) * steps + lax.div(row, SUB), 1.0, 0.0)
     swap = swap.astype(jnp.bfloat16)
     for n in range(src.shape[1] // 256):
@@ -121,9 +138,9 @@
     tok, gain, win, taps, conv_bias, recur_gate, recur_bias, input_gate, input_bias, setting,
     spikes, wout, out,
     win_all, wout_all, gates_all, vec_all, spike_all, raw, home, act, final, tails, pasts,
-    scaled, states,
-    y_recv, x_recv, d_recv, y_send, x_send, d_send, own_sem,
-    small_recv, small_send, raw_sem, act_recv, act_send, home_sem, out_recv,
+    scaled, power, states,
+    y_recv, x_recv, d_recv, g_recv, y_send, x_send, d_send, g_send, own_sem,
+    small_recv, small_send, raw_sem, act_recv, act_send, home_sem, out_recv, lag_sem,
 ):
     position = lax.axis_index("pp")
     x = lax.axis_index("fs")
@@ -132,7 +149,7 @@
     y = lax.rem(position, PLANE)
     parity = lax.rem(x, 2)
     length, width = raw.shape
-    inner = win_all.shape[2]
+    inner = wout_all.shape[2]
     chunk = length // HALVES
 
     def at_y(by):
@@ -150,12 +167,10 @@
     z_peers = [{"pp": lax.rem(z + by, planes) * PLANE + y} for by in range(1, planes)]
 
     own = [
-        pltpu.make_async_copy(recur_gate.at[0], gates_all.at[y, :, :, pl.ds(0, 128)], own_sem.at[0]),
-        pltpu.make_async_copy(input_gate.at[0], gates_all.at[y, :, :, pl.ds(128, 128)], own_sem.at[1]),
-        pltpu.make_async_copy(win.at[0], win_all.at[y], own_sem.at[2]),
-        pltpu.make_async_copy(wout.at[0], wout_all.at[y], own_sem.at[3]),
+        pltpu.make_async_copy(source.at[0], gates_all.at[y, n], own_sem.at[n])
+        for n, source in enumerate((recur_gate, input_gate))
     ]
-    for copy in own[:2]:
+    for copy in own:
         copy.start()
     pltpu.make_async_copy(tok.at[0, 0], raw, raw_sem).start()
 
@@ -166,66 +181,72 @@
 
     vec_all[y, 0:1] = gain[:, :inner]
     vec_all[y, 1:2] = gain[:, inner:]
-    vec_all[y, 2:6] = taps[0]
-    vec_all[y, 6:7] = conv_bias[...]
-    vec_all[y, 7:8] = recur_bias[...]
-    vec_all[y, 8:9] = input_bias[...]
+    log2e = 1.4426950408889634
+    vec_all[y, 2:6] = 0.5 * taps[0]
+    vec_all[y, 6:7] = 0.5 * conv_bias[...]
+    vec_all[y, 7:8] = 0.5 * recur_bias[...]
+    vec_all[y, 8:9] = 0.5 * input_bias[...]
     below = -setting[...]
-    vec_all[y, 9:10] = -8.0 * (jnp.maximum(below, 0.0) + jnp.log1p(jnp.exp(-jnp.abs(below))))
+    softplus = jnp.maximum(below, 0.0) + jnp.log1p(jnp.exp(-jnp.abs(below)))
+    vec_all[y, 9:10] = (-4.0 * log2e) * softplus
     row = lax.broadcasted_iota(jnp.int32, (length, length), 0)
     col = lax.broadcasted_iota(jnp.int32, (length, length), 1)
     within = lax.rem(row, chunk)
     token = (row - within) + lax.rem(within, SUB) * (chunk // SUB) + lax.div(within, SUB)
     picked = jnp.sum(jnp.where(col == token, spikes[...], 0.0), axis=1, keepdims=True)
-    spike_all[y] = jnp.broadcast_to(picked, (length, 128))
+    spike_all[y] = jnp.broadcast_to(picked * log2e, (length, 128))
 
     pl.semaphore_wait(barrier, len(peers))
 
-    gathered = (win_all, wout_all, gates_all)
-
-    def piece(ref, a, index):
-        if a == 2:
-            return ref.at[index // 2, pl.ds(pl.multiple_of(lax.rem(index, 2) * 64, 64), 64)]
-        height = win_all.shape[1] // PARTS if a == 0 else wout_all.shape[1] // PARTS
-        return ref.at[pl.ds(pl.multiple_of(index * height, height), height)]
+    gathered = (win_all, wout_all)
+
+    def piece(a, slot, index):
+        if a == 1:
+            return wout_all.at[slot, index]
+        half = win_all.shape[2] // 2
+        return win_all.at[slot, index // 2, pl.ds(pl.multiple_of(lax.rem(index, 2) * half, half), half)]
+
+    def source(a, index):
+        if a == 1:
+            return wout.at[0, :, pl.ds(pl.multiple_of(index * 128, 128), 128)]
+        half = win_all.shape[2] // 2
+        return win.at[
+            0,
+            pl.ds(pl.multiple_of(lax.rem(index, 2) * half, half), half),
+            pl.ds(pl.multiple_of(index // 2 * 128, 128), 128),
+        ]
+
+    def gate_piece(slot, index):
+        return gates_all.at[slot, :, pl.ds(4 * core + 2 * index, 2)]
+
+    def push(src, dst, send_sem, recv_sem, to):
+        pltpu.make_async_remote_copy(
+            src_ref=src, dst_ref=dst, send_sem=send_sem, recv_sem=recv_sem,
+            device_id=to, device_id_type=MESH,
+        ).start()
 
     def send(a, src, slot, index, send_sem, recv_sem, to):
-        pltpu.make_async_remote_copy(
-            src_ref=src,
-            dst_ref=piece(gathered[a].at[slot], a, index),
-            send_sem=send_sem,
-            recv_sem=recv_sem,
-            device_id=to,
-            device_id_type=MESH,
-        ).start()
+        push(src, piece(a, slot, index), send_sem, recv_sem, to)
 
     def await_bytes(ref, sem):
         pltpu.make_async_copy(ref, ref, sem).wait()
 
     def pieces_of(a, count):
-        if a == 2:
-            if count <= PARTS:
-                return gates_all.at[0, pl.ds(0, count // 2)]
-            return gates_all.at[pl.ds(0, 2), pl.ds(0, count // 4)]
-        height = gathered[a].shape[1] // PARTS
-        if count <= PARTS:
-            return gathered[a].at[0, pl.ds(0, count * height)]
-        return gathered[a].at[pl.ds(0, 2), pl.ds(0, count // 2 * height)]
+        tiles = count // 2 if a == 0 else count
+        if count == 6:
+            return gathered[a].at[0, pl.ds(0, tiles)]
+        return gathered[a].at[pl.ds(0, 2), pl.ds(0, tiles // 2)]
 
     mine = 8 * parity + 4 * core
     other = 8 * (1 - parity) + 4 * core
 
     for unit in range(4):
-        for a in range(3):
-            if unit == 0 and a == 2:
-                for copy in own[:2]:
-                    copy.wait()
-            source = (win.at[0], wout.at[0], gates_all.at[y])[a]
+        for a in range(2):
             j = unit
-            send(a, piece(source, a, mine + j), y, mine + j,
+            send(a, source(a, mine + j), y, mine + j,
                  y_send.at[0, a], y_recv.at[0, unit, a], up)
             j = (unit + 2) % 4
-            send(a, piece(source, a, mine + j), y, mine + j,
+            send(a, source(a, mine + j), y, mine + j,
                  y_send.at[1, a], y_recv.at[1, unit, a], down)
     smalls = (vec_all, spike_all)
     for n, ref in enumerate(smalls):
@@ -235,13 +256,19 @@
                 recv_sem=small_recv.at[n, by - 1],
                 device_id={"pp": at_y(by)}, device_id_type=MESH,
             ).start()
-    for copy in own[2:]:
-        copy.start()
+    for n in range(win_all.shape[1]):
+        pltpu.make_async_copy(
+            win.at[0, :, n * 128 : (n + 1) * 128], win_all.at[y, n], own_sem.at[2]
+        ).start()
+    for n in range(wout_all.shape[1]):
+        pltpu.make_async_copy(
+            wout.at[0, :, n * 128 : (n + 1) * 128], wout_all.at[y, n], own_sem.at[3]
+        ).start()
 
     await_bytes(raw, raw_sem)
     for half in range(HALVES):
         rows = slice(half * chunk, (half + 1) * chunk)
-        reorder(raw.at[rows], home.at[rows])
+        reorder(raw.at[rows], home.at[rows], False)
 
         @pl.when(z != 0)
         def _():
@@ -267,7 +294,7 @@
 
     def relay_y(unit, a):
         for side, (slot, j) in enumerate(arrivals(unit)):
-            ref = piece(gathered[a].at[slot], a, mine + j)
+            ref = piece(a, slot, mine + j)
             await_bytes(ref, y_recv.at[side, unit, a])
             if unit < 2:
                 send(a, ref, slot, mine + j, y_send.at[side, a],
@@ -279,24 +306,45 @@
 
     def relay_x(unit, a):
         for side, (slot, j) in enumerate(x_units[unit]):
-            ref = piece(gathered[a].at[slot], a, other + j)
+            ref = piece(a, slot, other + j)
             await_bytes(ref, x_recv.at[side, unit, a])
             send(a, ref, slot, other + j, d_send.at[a], d_recv.at[a], sibling)
 
-    for unit in range(7):
-        for a in range(3):
-            if unit < 6:
-                relay_y(unit, a)
+    def relay_gates(n):
+        slots = ((3, 0), (3, 1), (2, 0)), ((1, 1), (1, 0), (2, 1))
+        for side in range(2):
+            by, index = slots[side][n]
+            ref = gate_piece(plane_slot(by), index)
+            await_bytes(ref, g_recv.at[side, n])
+            if n == 0:
+                push(ref, ref, g_send.at[side], g_recv.at[side, 2], up if side == 0 else down)
+            push(ref, ref, d_send.at[2], d_recv.at[2], sibling)
+
+    for unit in range(6):
+        for a in range(2):
+            relay_y(unit, a)
             if unit > 0:
                 relay_x(unit - 1, a)
-
-    for copy in own[2:]:
-        copy.wait()
+        if unit == 1:
+            for copy in own:
+                copy.wait()
+            for n in range(2):
+                for side, to in enumerate((up, down)):
+                    ref = gate_piece(y, n if side == 0 else 1 - n)
+                    push(ref, ref, g_send.at[side], g_recv.at[side, n], to)
+    for n in range(3):
+        relay_gates(n)
+    for a in range(2):
+        relay_x(5, a)
+
+    await_bytes(win_all.at[y], own_sem.at[2])
+    await_bytes(wout_all.at[y], own_sem.at[3])
     for n, ref in enumerate(smalls):
         for by in range(1, 4):
             await_bytes(ref.at[plane_slot(4 - by)], small_recv.at[n, by - 1])
-    for a in range(3):
+    for a in range(2):
         await_bytes(pieces_of(a, 24), d_recv.at[a])
+    await_bytes(gates_all.at[pl.ds(0, 3), :, pl.ds(0, 4)], d_recv.at[2])
 
     def micro(step, token):
         i = step // HALVES
@@ -310,9 +358,21 @@
             tails[...] = jnp.zeros_like(tails)
             pasts[...] = jnp.zeros_like(pasts)
 
+        @pl.when((z == 0) & (core == 1) & (step == 0))
+        def _():
+            pl.semaphore_wait(lag_sem, 1)
+
+        prepare(here, vec_all.at[0], scaled, power)
+
         def one(s, token):
             layer(here, win_all.at[s], wout_all.at[s], gates_all.at[s], vec_all.at[s],
-                  spike_all.at[s, rows], tails.at[s], pasts.at[s], scaled, states)
+                  vec_all.at[lax.rem(s + 1, PLANE)], spike_all.at[s, rows], tails.at[s],
+                  pasts.at[s], scaled, power, states)
+
+            @pl.when((z == 0) & (core == 0) & (step == 0) & (s == 2))
+            def _():
+                pl.semaphore_signal(lag_sem, inc=1, device_id=sibling, device_id_type=MESH)
+
             return token
 
         lax.fori_loop(0, PLANE, one, 0)
@@ -327,7 +387,7 @@
 
         @pl.when(z == planes - 1)
         def _():
-            reorder(here, final.at[i, rows])
+            reorder(here, final.at[i, rows], True)
 
             @pl.when(i < planes - 1)
             def _():
@@ -365,11 +425,14 @@
     for n, ref in enumerate(smalls):
         for by in range(1, 4):
             await_bytes(ref.at[y], small_send.at[n, by - 1])
-    for a in range(3):
-        for side in range(2):
+    for side in range(2):
+        for a in range(2):
             await_bytes(pieces_of(a, 6), y_send.at[side, a])
             await_bytes(pieces_of(a, 6), x_send.at[side, a])
+        await_bytes(gates_all.at[pl.ds(0, 3), :, pl.ds(0, 2)], g_send.at[side])
+    for a in range(2):
         await_bytes(pieces_of(a, 24), d_send.at[a])
+    await_bytes(gates_all.at[pl.ds(0, 3), :, pl.ds(0, 4)], d_send.at[2])
 
 
 def local(
@@ -401,9 +464,9 @@
         in_specs=[hbm, near, hbm, near, near, hbm, near, hbm, near, near, near, hbm],
         out_specs=hbm,
         scratch_shapes=[
-            pltpu.VMEM((PLANE, width, inner), bf16),
-            pltpu.VMEM((PLANE, inner, width), bf16),
-            pltpu.VMEM((PLANE, blocks, 128, 256), bf16),
+            pltpu.VMEM((PLANE, inner // 128, width, 128), bf16),
+            pltpu.VMEM((PLANE, width // 128, inner, 128), bf16),
+            pltpu.VMEM((PLANE, 2, blocks, 128, 128), bf16),
             pltpu.VMEM((PLANE, 16, inner), f32),
             pltpu.VMEM((PLANE, length, 128), f32),
             pltpu.VMEM((length, width), bf16),
@@ -413,13 +476,16 @@
             pltpu.VMEM((PLANE, 3 * SUB, inner), f32),
             pltpu.VMEM((PLANE, SUB, inner), f32),
             pltpu.VMEM((length // HALVES, width), bf16),
+            pltpu.VMEM((length // HALVES, 128), f32),
             pltpu.VMEM((length // HALVES, inner), bf16),
-            dma((2, 6, 3)),
-            dma((2, 6, 3)),
+            dma((2, 6, 2)),
+            dma((2, 6, 2)),
             dma((3,)),
             dma((2, 3)),
-            dma((2, 3)),
+            dma((2, 2)),
+            dma((2, 2)),
             dma((3,)),
+            dma((2,)),
             dma((4,)),
             dma((2, 3)),
             dma((2, 3)),
@@ -428,6 +494,7 @@
             dma((planes, HALVES)),
             dma((HALVES,)),
             dma((HALVES,)),
+            pltpu.SemaphoreType.REGULAR,
         ],
         compiler_params=pltpu.CompilerParams(
             collective_id=0, has_side_effects=True, vmem_limit_bytes=60 * 1024 * 1024

time: 211 us -> 197 us (0.934)
  Pallas kernels: 208 us -> 195 us
    pallas_call x1, Pallas kernels: 208 us -> 195 us  [local(): pl.pallas_call(functools.partial(kernel, planes, columns), out_shape=jax....]
where the time goes in v3:
time: 197 us
  Pallas kernels  195 us (99%)
    pallas_call x1, Pallas kernels, local(): pl.pallas_call(functools.partial(kernel, planes, columns), out_shape=jax....  195 us

profile of v3, /device:TPU:97, one launch (start us, length us, event | category | flops | bytes accessed | tf_op | source)
XLA Modules:
  0.0 196.6 jit_solution(9897534293300636979)
XLA Ops:
  0.0 194.8 %shard_map.118 = bf16[1,1,128,2048]{3,2,1,0:T(8,128)(2,1)} custom-call(bf16[1,1,128,2048]{3,2,1,0:T(8,128)(2,1)} %tok.1, f32[1,2048]{1,0:T(1,128)} %gain.1, bf16[1,2048,1024]{2,1,0:T(8,128)(2,1)} %win.1, f32[1,4,1024]{2,1,0:T(4,128)} %taps.1, f32[1,1024]{1,0:T(1,128)} %conv_bias.1, bf16[1,8,128,128]{3,2,1,0:T(8,128)(2,1)} %recur_gate.1, ...), custom_call_target="tpu_custom_call" | custom-call | tf_op jit(solution)/shard_map/pallas_call | solution.py:461
  194.8 1.9 copy.14

commit v4 on v3

--- a/solution.py
+++ b/solution.py
@@ -138,9 +138,11 @@
     tok, gain, win, taps, conv_bias, recur_gate, recur_bias, input_gate, input_bias, setting,
     spikes, wout, out,
     win_all, wout_all, gates_all, vec_all, spike_all, raw, home, act, final, tails, pasts,
-    scaled, power, states,
+    scaled, power, states, relay_wout, relay_gate,
+    onward_wout, onward_gate,
     y_recv, x_recv, d_recv, g_recv, y_send, x_send, d_send, g_send, own_sem,
     small_recv, small_send, raw_sem, act_recv, act_send, home_sem, out_recv, lag_sem,
+    f_send, f_recv, h_send, h_recv, k_send, k_recv,
 ):
     position = lax.axis_index("pp")
     x = lax.axis_index("fs")
@@ -175,7 +177,8 @@
     pltpu.make_async_copy(tok.at[0, 0], raw, raw_sem).start()
 
     barrier = pltpu.get_barrier_semaphore()
-    peers = [up, down, across, right, left, sibling] + z_peers
+    mirror = [{"pp": (planes - 1 - z) * PLANE + lax.rem(y + by, PLANE)} for by in range(1, 4)]
+    peers = [up, down, across, right, left, sibling] + z_peers + mirror
     for peer in peers:
         pl.semaphore_signal(barrier, inc=1, device_id=peer, device_id_type=MESH)
 
@@ -240,14 +243,75 @@
     mine = 8 * parity + 4 * core
     other = 8 * (1 - parity) + 4 * core
 
-    for unit in range(4):
+    first, last = z == 0, z == planes - 1
+    lower = pl.ds(wout_all.shape[2] // 2, wout_all.shape[2] // 2)
+    upper = pl.ds(0, wout_all.shape[2] // 2)
+    detours = [(8 * side + 4 * core + j) for side in range(2) for j in (1, 3)]
+    core_gates = pl.ds(4 * core, 4)
+
+    for copy in own:
+        copy.wait()
+
+    @pl.when(first)
+    def _():
+        to = {"pp": (planes - 1) * PLANE + y}
+        for n, index in enumerate(detours):
+            column = pl.ds(pl.multiple_of(index * 128, 128), 128)
+            push(wout.at[0, lower, column], relay_wout.at[n], f_send.at[0], f_recv.at[n], to)
+        push(gates_all.at[y, :, core_gates], relay_gate, f_send.at[1], f_recv.at[4], to)
+
+    def split(a, j, act_on):
+        if a == 0 or j % 2 == 0:
+            act_on(lambda ref: ref)
+            return
+
+        @pl.when(first)
+        def _():
+            act_on(lambda ref: ref.at[upper])
+
+        @pl.when(z != 0)
+        def _():
+            act_on(lambda ref: ref)
+
+    def start_unit(unit):
         for a in range(2):
-            j = unit
-            send(a, source(a, mine + j), y, mine + j,
-                 y_send.at[0, a], y_recv.at[0, unit, a], up)
-            j = (unit + 2) % 4
-            send(a, source(a, mine + j), y, mine + j,
-                 y_send.at[1, a], y_recv.at[1, unit, a], down)
+            for side, to in enumerate((up, down)):
+                j = (unit + 2 * side) % 4
+                split(a, j, lambda cut: push(
+                    cut(source(a, mine + j)), cut(piece(a, y, mine + j)),
+                    y_send.at[side, a], y_recv.at[side, unit, a], to))
+
+    start_unit(0)
+
+    def detour(slot, n):
+        return wout_all.at[slot, detours[n], lower] if n < 4 else gates_all.at[slot, :, core_gates]
+
+    headings = (3, 1, 1, 1, 3)
+
+    @pl.when(last)
+    def _():
+        for n, heading in enumerate(headings):
+            ref, store = (relay_wout.at[n], onward_wout.at[n]) if n < 4 else (relay_gate, onward_gate)
+            await_bytes(ref, f_recv.at[n])
+            push(ref, store, k_send.at[n // 4], k_recv.at[n], {"pp": at_y(heading)})
+            by = 4 - heading
+            push(ref, detour(y, n), h_send.at[n // 4], h_recv.at[by - 1, n],
+                 {"pp": lax.rem(y + by, PLANE)})
+
+    start_unit(1)
+
+    @pl.when(last)
+    def _():
+        for n, heading in enumerate(headings):
+            ref = onward_wout.at[n] if n < 4 else onward_gate
+            await_bytes(ref, k_recv.at[n])
+            dst = detour(plane_slot(4 - heading), n)
+            push(ref, dst, h_send.at[n // 4], h_recv.at[1, n],
+                 {"pp": lax.rem(y + heading, PLANE)})
+            push(ref, dst, h_send.at[n // 4], h_recv.at[heading - 1, n], {"pp": y})
+
+    start_unit(2)
+    start_unit(3)
     smalls = (vec_all, spike_all)
     for n, ref in enumerate(smalls):
         for by in range(1, 4):
@@ -270,17 +334,16 @@
         rows = slice(half * chunk, (half + 1) * chunk)
         reorder(raw.at[rows], home.at[rows], False)
 
-        @pl.when(z != 0)
-        def _():
-            pltpu.make_async_remote_copy(
-                src_ref=home.at[rows], dst_ref=act.at[z, rows], send_sem=home_sem.at[half],
-                recv_sem=act_recv.at[z, half],
-                device_id={"pp": y}, device_id_type=MESH,
-            ).start()
-
         @pl.when(z == 0)
         def _():
             pltpu.make_async_copy(home.at[rows], act.at[0, rows], act_recv.at[0, half]).start()
+
+    def send_home():
+        for half in range(HALVES):
+            rows = slice(half * chunk, (half + 1) * chunk)
+            push(home.at[rows], act.at[z, rows], home_sem.at[half], act_recv.at[z, half], {"pp": y})
+
+    pl.when((z == 1) | last)(send_home)
 
     def arrivals(unit):
         from_below = (plane_slot(3), unit) if unit < 4 else (plane_slot(2), unit - 4)
@@ -294,21 +357,27 @@
 
     def relay_y(unit, a):
         for side, (slot, j) in enumerate(arrivals(unit)):
-            ref = piece(a, slot, mine + j)
-            await_bytes(ref, y_recv.at[side, unit, a])
-            if unit < 2:
-                send(a, ref, slot, mine + j, y_send.at[side, a],
-                     y_recv.at[side, 4 + unit, a], up if side == 0 else down)
-            x_side = 0 if j < 2 else 1
-            send(a, ref, slot, mine + j, x_send.at[x_side, a],
-                 x_recv.at[x_side, unit, a], left if x_side == 0 else right)
-            send(a, ref, slot, mine + j, d_send.at[a], d_recv.at[a], sibling)
+            def forward(cut):
+                ref = cut(piece(a, slot, mine + j))
+                await_bytes(ref, y_recv.at[side, unit, a])
+                if unit < 2:
+                    push(ref, ref, y_send.at[side, a], y_recv.at[side, 4 + unit, a],
+                         up if side == 0 else down)
+                x_side = 0 if j < 2 else 1
+                push(ref, ref, x_send.at[x_side, a], x_recv.at[x_side, unit, a],
+                     left if x_side == 0 else right)
+                push(ref, ref, d_send.at[a], d_recv.at[a], sibling)
+
+            split(a, j, forward)
 
     def relay_x(unit, a):
         for side, (slot, j) in enumerate(x_units[unit]):
-            ref = piece(a, slot, other + j)
-            await_bytes(ref, x_recv.at[side, unit, a])
-            send(a, ref, slot, other + j, d_send.at[a], d_recv.at[a], sibling)
+            def forward(cut):
+                ref = cut(piece(a, slot, other + j))
+                await_bytes(ref, x_recv.at[side, unit, a])
+                push(ref, ref, d_send.at[a], d_recv.at[a], sibling)
+
+            split(a, j, forward)
 
     def relay_gates(n):
         slots = ((3, 0), (3, 1), (2, 0)), ((1, 1), (1, 0), (2, 1))
@@ -325,15 +394,30 @@
             relay_y(unit, a)
             if unit > 0:
                 relay_x(unit - 1, a)
+        if unit == 4:
+            pl.when((z > 1) & (z != planes - 1))(send_home)
         if unit == 1:
-            for copy in own:
-                copy.wait()
-            for n in range(2):
-                for side, to in enumerate((up, down)):
-                    ref = gate_piece(y, n if side == 0 else 1 - n)
-                    push(ref, ref, g_send.at[side], g_recv.at[side, n], to)
-    for n in range(3):
-        relay_gates(n)
+            @pl.when(z != 0)
+            def _():
+                for n in range(2):
+                    for side, to in enumerate((up, down)):
+                        ref = gate_piece(y, n if side == 0 else 1 - n)
+                        push(ref, ref, g_send.at[side], g_recv.at[side, n], to)
+
+    @pl.when(z != 0)
+    def _():
+        for n in range(3):
+            relay_gates(n)
+
+    @pl.when(first)
+    def _():
+        for n in range(5):
+            for by in range(1, 4):
+                slot = plane_slot(4 - by)
+                ref = detour(slot, n)
+                await_bytes(ref, h_recv.at[by - 1, n])
+                push(ref, ref, d_send.at[1 + n // 4], d_recv.at[1 + n // 4], sibling)
+
     for a in range(2):
         relay_x(5, a)
 
@@ -426,10 +510,33 @@
         for by in range(1, 4):
             await_bytes(ref.at[y], small_send.at[n, by - 1])
     for side in range(2):
-        for a in range(2):
-            await_bytes(pieces_of(a, 6), y_send.at[side, a])
-            await_bytes(pieces_of(a, 6), x_send.at[side, a])
-        await_bytes(gates_all.at[pl.ds(0, 3), :, pl.ds(0, 2)], g_send.at[side])
+        for sem in (y_send, x_send):
+            await_bytes(pieces_of(0, 6), sem.at[side, 0])
+
+            @pl.when(first)
+            def _():
+                await_bytes(wout_all.at[0, pl.ds(0, 9), upper], sem.at[side, 1])
+
+            @pl.when(z != 0)
+            def _():
+                await_bytes(pieces_of(1, 6), sem.at[side, 1])
+
+        @pl.when(z != 0)
+        def _():
+            await_bytes(gates_all.at[pl.ds(0, 3), :, pl.ds(0, 2)], g_send.at[side])
+
+    @pl.when(first)
+    def _():
+        await_bytes(relay_wout, f_send.at[0])
+        await_bytes(relay_gate, f_send.at[1])
+
+    @pl.when(last)
+    def _():
+        await_bytes(onward_wout, k_send.at[0])
+        await_bytes(onward_gate, k_send.at[1])
+        await_bytes(wout_all.at[0, pl.ds(0, 12), upper], h_send.at[0])
+        await_bytes(gates_all.at[pl.ds(0, 3), :, pl.ds(0, 4)], h_send.at[1])
+
     for a in range(2):
         await_bytes(pieces_of(a, 24), d_send.at[a])
     await_bytes(gates_all.at[pl.ds(0, 3), :, pl.ds(0, 4)], d_send.at[2])
@@ -478,6 +585,10 @@
             pltpu.VMEM((length // HALVES, width), bf16),
             pltpu.VMEM((length // HALVES, 128), f32),
             pltpu.VMEM((length // HALVES, inner), bf16),
+            pltpu.VMEM((4, inner // 2, 128), bf16),
+            pltpu.VMEM((2, 4, 128, 128), bf16),
+            pltpu.VMEM((4, inner // 2, 128), bf16),
+            pltpu.VMEM((2, 4, 128, 128), bf16),
             dma((2, 6, 2)),
             dma((2, 6, 2)),
             dma((3,)),
@@ -495,6 +606,12 @@
             dma((HALVES,)),
             dma((HALVES,)),
             pltpu.SemaphoreType.REGULAR,
+            dma((2,)),
+            dma((5,)),
+            dma((2,)),
+            dma((3, 5)),
+            dma((2,)),
+            dma((5,)),
         ],
         compiler_params=pltpu.CompilerParams(
             collective_id=0, has_side_effects=True, vmem_limit_bytes=60 * 1024 * 1024

time: 197 us -> 188 us (0.954)
  Pallas kernels: 195 us -> 186 us
    pallas_call x1, Pallas kernels: 195 us -> 186 us  [local(): pl.pallas_call(functools.partial(kernel, planes, columns), out_shape=jax....]
where the time goes in v4:
time: 188 us; the launch traced here: 187 us
  Pallas kernels  186 us (99%)
    pallas_call x1, Pallas kernels, local(): pl.pallas_call(functools.partial(kernel, planes, columns), out_shape=jax....  186 us

profile of v4, /device:TPU:97, one launch (start us, length us, event | category | flops | bytes accessed | tf_op | source)
XLA Modules:
  0.0 187.5 jit_solution(5642783855603787401)
XLA Ops:
  0.0 185.6 %shard_map.118 = bf16[1,1,128,2048]{3,2,1,0:T(8,128)(2,1)} custom-call(bf16[1,1,128,2048]{3,2,1,0:T(8,128)(2,1)} %tok.1, f32[1,2048]{1,0:T(1,128)} %gain.1, bf16[1,2048,1024]{2,1,0:T(8,128)(2,1)} %win.1, f32[1,4,1024]{2,1,0:T(4,128)} %taps.1, f32[1,1024]{1,0:T(1,128)} %conv_bias.1, bf16[1,8,128,128]{3,2,1,0:T(8,128)(2,1)} %recur_gate.1, ...), custom_call_target="tpu_custom_call" | custom-call | tf_op jit(solution)/shard_map/pallas_call | solution.py:568
  185.6 1.9 %copy.14 = bf16[1,1,128,2048]{3,2,1,0:T(8,128)(2,1)} copy(bf16[1,1,128,2048]{3,2,1,0:T(8,128)(2,1)} %shard_map.118) | data formatting | bytes 1048576

commit v5 on v4

--- a/solution.py
+++ b/solution.py
@@ -89,17 +89,18 @@
         states[:, cols] = done.reshape(length, 128).astype(jnp.bfloat16)
 
     groups = inner // 256
-    mixed = project(0)
+    first_mixed = project(0)
     scale = lax.rsqrt(jnp.sum(power[...], axis=1, keepdims=True) * (1.0 / width) + 1e-6)
     scale = jnp.broadcast_to(scale, (length, 128))
     spikes = spike[...].reshape(steps, SUB, 128)
+    queue = [first_mixed, project(1)]
     for n in range(groups):
-        later = project(n + 1) if n + 1 < groups else None
-        left = conv_of(mixed[:, :128], 2 * n)
-        right = conv_of(mixed[:, 128:], 2 * n + 1)
+        if n + 2 < groups:
+            queue.append(project(n + 2))
+        left = conv_of(queue[n][:, :128], 2 * n)
+        right = conv_of(queue[n][:, 128:], 2 * n + 1)
         recur(*left, 2 * n)
         recur(*right, 2 * n + 1)
-        mixed = later
 
     total = jnp.zeros((length, 128), jnp.float32)
     for m in range(width // 256):
@@ -569,7 +570,7 @@
         functools.partial(kernel, planes, columns),
         out_shape=jax.ShapeDtypeStruct(tokens.shape, bf16),
         in_specs=[hbm, near, hbm, near, near, hbm, near, hbm, near, near, near, hbm],
-        out_specs=hbm,
+        out_specs=near,
         scratch_shapes=[
             pltpu.VMEM((PLANE, inner // 128, width, 128), bf16),
             pltpu.VMEM((PLANE, width // 128, inner, 128), bf16),

time: 188 us -> 186 us (0.989)
  Pallas kernels: 186 us -> 184 us
where the time goes in v5:
time: 186 us
  Pallas kernels  184 us (99%)
  local copies, waits for them, and re-layouts  1.88 us (1%)
    pallas_call x1, Pallas kernels, local(): pl.pallas_call(functools.partial(kernel, planes, columns), out_shape=jax....  184 us

profile of v5, /device:TPU:97, one launch (start us, length us, event | category | flops | bytes accessed | tf_op | source)
XLA Modules:
  0.0 185.7 jit_solution(9052754377804572866)
XLA Ops:
  0.0 183.8 %shard_map.118 = bf16[1,1,128,2048]{3,2,1,0:T(8,128)(2,1)} custom-call(bf16[1,1,128,2048]{3,2,1,0:T(8,128)(2,1)} %tok.1, f32[1,2048]{1,0:T(1,128)} %gain.1, bf16[1,2048,1024]{2,1,0:T(8,128)(2,1)} %win.1, f32[1,4,1024]{2,1,0:T(4,128)} %taps.1, f32[1,1024]{1,0:T(1,128)} %conv_bias.1, bf16[1,8,128,128]{3,2,1,0:T(8,128)(2,1)} %recur_gate.1, ...), custom_call_target="tpu_custom_call" | custom-call | tf_op jit(solution)/shard_map/pallas_call | solution.py:569
  183.8 1.9 %copy.14 = bf16[1,1,128,2048]{3,2,1,0:T(8,128)(2,1)} copy(bf16[1,1,128,2048]{3,2,1,0:T(8,128)(2,1)} %shard_map.118) | data formatting | bytes 1048576

commit v6 on v5

--- a/solution.py
+++ b/solution.py
@@ -250,16 +250,12 @@
     detours = [(8 * side + 4 * core + j) for side in range(2) for j in (1, 3)]
     core_gates = pl.ds(4 * core, 4)
 
-    for copy in own:
-        copy.wait()
-
     @pl.when(first)
     def _():
         to = {"pp": (planes - 1) * PLANE + y}
         for n, index in enumerate(detours):
             column = pl.ds(pl.multiple_of(index * 128, 128), 128)
             push(wout.at[0, lower, column], relay_wout.at[n], f_send.at[0], f_recv.at[n], to)
-        push(gates_all.at[y, :, core_gates], relay_gate, f_send.at[1], f_recv.at[4], to)
 
     def split(a, j, act_on):
         if a == 0 or j % 2 == 0:
@@ -283,6 +279,14 @@
                     y_send.at[side, a], y_recv.at[side, unit, a], to))
 
     start_unit(0)
+
+    for copy in own:
+        copy.wait()
+
+    @pl.when(first)
+    def _():
+        to = {"pp": (planes - 1) * PLANE + y}
+        push(gates_all.at[y, :, core_gates], relay_gate, f_send.at[1], f_recv.at[4], to)
 
     def detour(slot, n):
         return wout_all.at[slot, detours[n], lower] if n < 4 else gates_all.at[slot, :, core_gates]

time: 186 us -> 186 us (level)
  no operation moved by 1% of the time
where the time goes in v6:
time: 186 us
  Pallas kernels  184 us (99%)
  local copies, waits for them, and re-layouts  1.88 us (1%)
    pallas_call x1, Pallas kernels, local(): pl.pallas_call(functools.partial(kernel, planes, columns), out_shape=jax....  184 us

profile of v6, /device:TPU:97, one launch (start us, length us, event | category | flops | bytes accessed | tf_op | source)
XLA Modules:
  0.0 185.7 jit_solution(5333532122011371181)
XLA Ops:
  0.0 183.8 %shard_map.118 = bf16[1,1,128,2048]{3,2,1,0:T(8,128)(2,1)} custom-call(bf16[1,1,128,2048]{3,2,1,0:T(8,128)(2,1)} %tok.1, f32[1,2048]{1,0:T(1,128)} %gain.1, bf16[1,2048,1024]{2,1,0:T(8,128)(2,1)} %win.1, f32[1,4,1024]{2,1,0:T(4,128)} %taps.1, f32[1,1024]{1,0:T(1,128)} %conv_bias.1, bf16[1,8,128,128]{3,2,1,0:T(8,128)(2,1)} %recur_gate.1, ...), custom_call_target="tpu_custom_call" | custom-call | tf_op jit(solution)/shard_map/pallas_call | solution.py:573
  183.8 1.9 %copy.14 = bf16[1,1,128,2048]{3,2,1,0:T(8,128)(2,1)} copy(bf16[1,1,128,2048]{3,2,1,0:T(8,128)(2,1)} %shard_map.118) | data formatting | bytes 1048576
